TPU v7x, 512 devices: a whole 4x8x8 slice. The times are simulated.
512 devices in a mesh: sp: 64 (over z, y), tp: 8 (over x, core).
Axes of the slice: x: 4, y: 8, z: 8, core: 2. Of those that a mesh axis runs over, the one named last changes fastest.
Arguments:
- resid: bfloat16 [24576, 2048], P('sp'), may hold values from -6 to 6
- x_branch: bfloat16 [24576, 2048], P('sp', 'tp'), may hold values from -6 to 6
- gate_branch: bfloat16 [24576, 2048], P('sp', 'tp'), may hold values from -6 to 6
- conv_w: float32 [4, 2048], P(None, 'tp'), may hold values from -3 to 3
- gate_a_w: bfloat16 [32, 64, 64], P('tp'), may hold values from -0.75 to 0.75
- gate_x_w: bfloat16 [32, 64, 64], P('tp'), may hold values from -0.75 to 0.75
- decay_rate: float32 [2048], P('tp'), may hold values from 0 to 0.01, as said below
- decay_extra: float32 [24576, 2048], P('sp', 'tp'), may hold values from -3 to 0, as said below
- w_proj: bfloat16 [2048, 2048], P('tp'), may hold values from -0.125 to 0.125
- mix_gain: float32 [2048], replicated, may hold values from 0.1 to 1.9
- pre_gain: float32 [2048], replicated, may hold values from 0.1 to 1.9
- w_gate: bfloat16 [2048, 5632], P('sp', 'tp'), may hold values from -0.125 to 0.125
- w_up: bfloat16 [2048, 5632], P('sp', 'tp'), may hold values from -0.125 to 0.125
- w_down: bfloat16 [5632, 2048], P('tp', 'sp'), may hold values from -0.078125 to 0.078125
- out_gain: float32 [2048], replicated, may hold values from 0.1 to 1.9
Outputs:
- stream_out: bfloat16 [24576, 2048], P(('sp', 'tp'))
Inputs may be any that keep to these rules, and one draw needn't show every extreme that they name: `decay_rate`: positive rates. `decay_extra`: non-positive values.
All inputs are finite; a program needn't handle non-finite values.
Results may differ from a plain program's by a relative error of at most 0.015.
Values may be sent and summed in bfloat16 or wider, within the bound.
A program may use at most 64 MiB of HBM per device.

v0:
```python
import jax
import jax.numpy as jnp
from jax import lax
from jax.sharding import Mesh
from jax.sharding import PartitionSpec as P

SP = ("sp_0", "sp_1")
SP_TP = ("sp_0", "sp_1", "tp")


LRU_SCALE = 8.0
NORM_EPS = 1e-06


def from_behind(value, axis, steps):
    count = lax.axis_size(axis)
    first, last = (max(0, -steps), min(count, count - steps))
    return lax.ppermute(value, axis, [(source, source + steps) for source in range(first, last)])


def nothing_yet(value, identity):
    return jax.tree.map(
        lambda part, zero: jnp.zeros_like(part) + jnp.asarray(zero, part.dtype), value, identity
    )


def gathered_once(value, axis):
    leaves = jax.tree.leaves(value)
    sequence = sorted(range(len(leaves)), key=lambda k: -leaves[k].size)
    width = (1, *leaves[sequence[0]].shape)[-1]
    lines = [
        jnp.pad(leaves[k].reshape(-1), (0, -leaves[k].size % width)).reshape(-1, width)
        for k in sequence
    ]
    both, at, found = (lax.all_gather(jnp.concatenate(lines), axis), 0, {})
    for k, line in zip(sequence, lines):
        share = both[:, at : at + len(line)].reshape(len(both), -1)
        found[k] = share[:, : leaves[k].size].reshape(-1, *leaves[k].shape)
        at += len(line)
    numbers = iter(range(len(leaves)))
    return jax.tree.map(lambda _: found[next(numbers)], value)


def entering(value, axes, combine, identity):
    before = start = nothing_yet(value, identity)
    so_far = value
    for axis in reversed(axes):
        devices, mine = (lax.axis_size(axis), lax.axis_index(axis))
        pieces = gathered_once(so_far, axis)
        inside, so_far = (start, start)
        for k in range(devices):
            passed = k < mine
            so_far = combine(so_far, jax.tree.map(lambda part: part[k], pieces))
            inside = jax.tree.map(lambda new, old: jnp.where(passed, new, old), so_far, inside)
        before = combine(inside, before)
    return before


def split_up(value, dim, devices):
    shape = value.shape
    pieces = value.reshape(*shape[:dim], devices, shape[dim] // devices, *shape[dim + 1 :])
    return jnp.moveaxis(pieces, dim, 0)


def sent_and_summed(value, axis, dim):
    pieces = split_up(value, dim, lax.axis_size(axis))
    arrived = lax.all_to_all(pieces, axis, split_axis=0, concat_axis=0, tiled=True)
    return arrived.astype(jnp.float32).sum(axis=0)


def joined_along(pieces, dim):
    pieces = jnp.moveaxis(pieces, 0, dim)
    shape = pieces.shape
    return pieces.reshape(*shape[:dim], shape[dim] * shape[dim + 1], *shape[dim + 2 :])


def copy_for_each(value, axis):
    devices = lax.axis_size(axis)
    return lax.all_to_all(
        jnp.broadcast_to(value[None], (devices, *value.shape)), axis, 0, 0, tiled=True
    )


def collect(value, axis, dim):
    return joined_along(copy_for_each(value, axis), dim)


def sent_together(arrays, axis, dim, along):
    ends, at = ([], 0)
    for a in arrays[:-1]:
        at += a.shape[along]
        ends.append(at)
    both = jnp.concatenate(arrays, axis=along)
    return tuple(jnp.split(lax.all_gather(both, axis, axis=dim, tiled=True), ends, axis=along))


def stacked_from(value, axes, sequence):
    pieces = value
    for k in sequence:
        pieces = lax.all_gather(pieces, axes[k])
    done = sequence[::-1]
    back = [done.index(k) for k in range(len(axes))]
    pieces = pieces.transpose(*back, *range(len(axes), pieces.ndim))
    return pieces.reshape(-1, *value.shape)


def gather_axes(value, axes, sequence, dim):
    return joined_along(stacked_from(value, axes, sequence), dim)


def chain(earlier, later):
    return (earlier[0] * later[0], later[0] * earlier[1] + later[1])


def rms_scale(values, gains):
    return values * lax.rsqrt(jnp.mean(values * values, axis=-1, keepdims=True) + NORM_EPS) * gains


def shards(
    resid,
    x_branch,
    gate_branch,
    conv_w,
    gate_a_w,
    gate_x_w,
    decay_rate,
    decay_extra,
    w_proj,
    mix_gain,
    pre_gain,
    w_gate,
    w_up,
    w_down,
    out_gain,
):
    length = x_branch.shape[0]
    width = x_branch.shape[1]
    taps = conv_w.shape[0]
    before = from_behind(x_branch[length - (taps - 1) :], SP, 1)
    padded = jnp.concatenate([before, x_branch], axis=0).astype(jnp.float32)
    conv = padded[0:length] * conv_w[0]
    for tap in range(1, taps):
        conv = conv + padded[tap : tap + length] * conv_w[tap]
    conv_out = conv.astype(jnp.bfloat16)
    nblocks = gate_a_w.shape[0]
    grouped = conv_out.reshape(length, nblocks, gate_a_w.shape[1])
    recur = jax.nn.sigmoid(
        jnp.einsum("rnc,ncd->rnd", grouped, gate_a_w, preferred_element_type=jnp.float32).reshape(
            length, width
        )
    )
    inject = jax.nn.sigmoid(
        jnp.einsum("rnc,ncd->rnd", grouped, gate_x_w, preferred_element_type=jnp.float32).reshape(
            length, width
        )
    )
    log_decay = -LRU_SCALE * recur * decay_rate + decay_extra
    decay = jnp.exp(log_decay)
    drive = jnp.sqrt(-jnp.expm1(2.0 * log_decay)) * inject * conv_out.astype(jnp.float32)
    prod_local, state_local = lax.associative_scan(chain, (decay, drive), axis=0)
    identity = (jnp.ones((width,), jnp.float32), jnp.zeros((width,), jnp.float32))
    carried = entering((prod_local[-1], state_local[-1]), SP, chain, identity)
    state = state_local + prod_local * carried[1][None, :]
    mixer = (state * jax.nn.gelu(gate_branch.astype(jnp.float32))).astype(jnp.bfloat16)
    share_rows = length // lax.axis_size("tp")
    first = lax.axis_index("tp") * share_rows
    mixed = sent_and_summed(
        jnp.dot(mixer, w_proj, preferred_element_type=jnp.float32).astype(jnp.bfloat16), "tp", 0
    )
    own_rows = lax.dynamic_slice_in_dim(resid, first, share_rows, 0).astype(jnp.float32)
    after_mix = own_rows + rms_scale(mixed, mix_gain)
    normed_own = rms_scale(after_mix, pre_gain).astype(jnp.bfloat16)
    normed = collect(normed_own, "tp", 0)
    gate_full, up_full = sent_together((w_gate, w_up), SP, 0, 1)
    down_full = gather_axes(w_down, SP, (0, 1), 1)
    gate = jnp.dot(normed, gate_full, preferred_element_type=jnp.float32)
    upward = jnp.dot(normed, up_full, preferred_element_type=jnp.float32)
    hidden = (jax.nn.silu(gate) * upward).astype(jnp.bfloat16)
    ffn = sent_and_summed(
        jnp.dot(hidden, down_full, preferred_element_type=jnp.float32).astype(jnp.bfloat16), "tp", 0
    )
    return (after_mix + 0.5 * rms_scale(ffn, out_gain)).astype(jnp.bfloat16)


def solution(mesh):
    finer = Mesh(mesh.devices.reshape(8, 8, mesh.shape["tp"]), ("sp_0", "sp_1", "tp"))
    return jax.shard_map(
        shards,
        mesh=finer,
        in_specs=(
            P(SP, None),
            P(SP, "tp"),
            P(SP, "tp"),
            P(None, "tp"),
            P("tp", None, None),
            P("tp", None, None),
            P("tp"),
            P(SP, "tp"),
            P("tp", None),
            P(),
            P(),
            P(SP, "tp"),
            P(SP, "tp"),
            P("tp", SP),
            P(),
        ),
        out_specs=P(SP_TP, None),
        check_vma=False,
    )
```

profile of v0, /device:TPU:1, one launch (start us, length us, event | category | flops | bytes accessed | tf_op | source)
XLA Modules:
  0.0 226.8 jit_solution(4761410293559854251)
XLA Ops:
  6.5 28.2 %all-gather.6 = bf16[8,704,32]{1,2,0:T(8,128)(2,1)} all-gather(bf16[1,704,32]{1,2,0:T(8,128)(2,1)} %bitcast.144), channel_id=4, replica_groups=mesh['sp_0'=8,'sp_1'=8,'tp'=8] {'sp_0'}, dimensions={0}, use_global_device_ids=true | all-gather | bytes 405504 | tf_op jit(solution)/shard_map/all_gather | solution.py:100
  34.8 0.7 slice.433
  35.5 3.2 %collective-permute-start = (bf16[3,256]{1,0:T(4,128)(2,1)S(1)}, bf16[3,256]{1,0:T(4,128)(2,1)S(1)}, u32[]{:S(2)}, u32[]{:S(2)}) collective-permute-start(bf16[3,256]{1,0:T(4,128)(2,1)S(1)} %slice.433), channel_id=1, source_target_pairs={{0,8},{8,16},{16,24},{24,32},{32,40},{40,48},{48,56},{56,64},{64,7... | collective-permute-start | bytes 4616 | tf_op jit(solution)/shard_map/ppermute | solution.py:18
  38.7 1.5 pad_maximum_fusion.4
  40.3 0.7 broadcast_multiply_fusion
  41.0 0.8 fusion.61
  41.8 1.0 maximum_convert_fusion
  44.5 0.5 convert_multiply_fusion.3
  48.9 20.8 %all-gather.4 = f32[8,2,256]{2,1,0:T(2,128)S(1)} all-gather(f32[1,2,256]{2,1,0:T(2,128)S(1)} %maximum_bitcast_fusion), channel_id=2, replica_groups=mesh['sp_0'=8,'sp_1'=8,'tp'=8] {'sp_1'}, dimensions={0}, use_global_device_ids=true | all-gather | bytes 18432 | tf_op jit(solution)/shard_map/all_gather | solution.py:35
  69.7 17.8 %all-gather.5 = f32[8,2,256]{2,1,0:T(2,128)S(1)} all-gather(f32[1,2,256]{2,1,0:T(2,128)S(1)} %maximum_bitcast_fusion.1), channel_id=3, replica_groups=mesh['sp_0'=8,'sp_1'=8,'tp'=8] {'sp_0'}, dimensions={0}, use_global_device_ids=true | all-gather | bytes 18432 | tf_op jit(solution)/shard_map/all_gather | solution.py:35
  87.6 1.9 convolution_convert_fusion.1
  89.5 19.2 %all-to-all-start = ((bf16[8,48,2048]{2,1,0:T(8,128)(2,1)}), bf16[8,48,2048]{2,1,0:T(8,128)(2,1)S(1)}, u32[]{:S(2)}, u32[]{:S(2)}) async-start(bf16[8,48,2048]{2,1,0:T(8,128)(2,1)} %bitcast.45), calls=%async_computation | async-start | bytes 3145728 | tf_op jit(solution)/shard_map/all_to_all | solution.py:67
  108.7 20.6 %all-to-all-done = bf16[8,48,2048]{2,1,0:T(8,128)(2,1)S(1)} async-done(((bf16[8,48,2048]{2,1,0:T(8,128)(2,1)}), bf16[8,48,2048]{2,1,0:T(8,128)(2,1)S(1)}, u32[]{:S(2)}, u32[]{:S(2)}) %all-to-all-start) | async-done | bytes 1572896 | tf_op jit(solution)/shard_map/all_to_all | solution.py:67
  129.7 1.2 multiply_reduce_fusion.1
  130.9 1.1 multiply_convert_fusion
  132.0 1.4 broadcast_in_dim.28
  133.4 4.5 %all-to-all-start.1 = ((bf16[8,48,2048]{2,1,0:T(8,128)(2,1)}), bf16[8,48,2048]{2,1,0:T(8,128)(2,1)S(1)}, u32[]{:S(2)}, u32[]{:S(2)}) async-start(bf16[8,48,2048]{2,1,0:T(8,128)(2,1)} %broadcast_in_dim.28), calls=%async_computation.1 | async-start | bytes 3145728 | tf_op jit(solution)/shard_map/all_to_all | solution.py:79
  137.8 3.8 %copy.117 = bf16[8,8,704,32]{2,3,1,0:T(8,128)(2,1)} copy(bf16[8,8,704,32]{2,3,0,1:T(8,128)(2,1)} %bitcast.135) | data formatting | bytes 5767168 | tf_op jit(solution)/shard_map/transpose | solution.py:103
  141.6 16.8 %all-to-all-done.1 = bf16[8,48,2048]{2,1,0:T(8,128)(2,1)S(1)} async-done(((bf16[8,48,2048]{2,1,0:T(8,128)(2,1)}), bf16[8,48,2048]{2,1,0:T(8,128)(2,1)S(1)}, u32[]{:S(2)}, u32[]{:S(2)}) %all-to-all-start.1) | async-done | bytes 1572896 | tf_op jit(solution)/shard_map/all_to_all | solution.py:79
  158.5 17.0 %all-gather.10.cloned.1.call-done = bf16[2048,1408]{1,0:T(8,128)(2,1)} async-done(((bf16[32,1408]{1,0:T(8,128)(2,1)}), bf16[2048,1408]{1,0:T(8,128)(2,1)}) %all-gather.10.cloned.1.call-update) | async-done | bytes 5767184 | tf_op jit(solution)/shard_map/all_gather | solution.py:94
  175.5 4.7 %fusion.2 = f32[384,704]{0,1:T(8,128)} fusion(bf16[384,2048]{1,0:T(8,128)(2,1)S(1)} %bitcast.137, bf16[2048,1408]{1,0:T(8,128)(2,1)} %all-gather.10.cloned.1.call-done), kind=kOutput, calls=%fused_computation.2 | convolution fusion | flops 1107296256 | bytes 5799936 | tf_op jit(solution)/shard_map/dot_general | solution.py:176
  180.1 8.6 %convolution_convert_fusion = bf16[384,2048]{1,0:T(8,128)(2,1)} fusion(bf16[704,2048]{0,1:T(8,128)(2,1)} %bitcast.136, bf16[384,2048]{1,0:T(8,128)(2,1)S(1)} %bitcast.138, bf16[2048,1408]{1,0:T(8,128)(2,1)} %all-gather.10.cloned.1.call-done, f32[384,704]{0,1:T(8,128)} %fusion.2), kind=kOutput, calls=%fused_computation.6 | convolution fusion | flops 2217000960 | bytes 10518528 | tf_op jit(solution)/shard_map/dot_general | solution.py:180
  188.7 28.8 %all_to_all.15 = bf16[8,48,2048]{2,1,0:T(8,128)(2,1)S(1)} all-to-all(bf16[8,48,2048]{2,1,0:T(8,128)(2,1)} %bitcast.139), channel_id=1, replica_groups=mesh['sp_0'=8,'sp_1'=8,'tp'=8] {'tp'}, dimensions={0} | all-to-all | bytes 3145728 | tf_op jit(solution)/shard_map/all_to_all | solution.py:67
  218.2 1.8 add_convert_fusion
  (174 shorter events, 6.0 us)
Async XLA Ops:
  6.5 81.1 %copy-start = (bf16[256,2048]{1,0:T(8,128)(2,1)S(1)}, bf16[256,2048]{1,0:T(8,128)(2,1)}, u32[]{:S(2)}) copy-start(bf16[256,2048]{1,0:T(8,128)(2,1)} %param.23) | copy-start | bytes 3145732
  6.5 131.3 %all-gather.12.cloned.1.call-start = ((), (), s32[]{:S(2)}) async-start(), calls=%async_computation.4 | async-start | bytes 3538944 | tf_op jit(solution)/shard_map/all_gather | solution.py:100
  34.7 8.4 %copy-start.6 = (bf16[4,64,64]{2,1,0:T(8,128)(2,1)S(1)}, bf16[4,64,64]{2,1,0:T(8,128)(2,1)}, u32[]{:S(2)}) copy-start(bf16[4,64,64]{2,1,0:T(8,128)(2,1)} %param.20) | copy-start | bytes 98308
  34.8 140.7 %all-gather.10.cloned.1.call-start = ((), (), s32[]{:S(2)}) async-start(), calls=%async_computation.3 | async-start | bytes 5857280 | tf_op jit(solution)/shard_map/all_gather | solution.py:94
  35.5 6.3 %collective-permute-start = (bf16[3,256]{1,0:T(4,128)(2,1)S(1)}, bf16[3,256]{1,0:T(4,128)(2,1)S(1)}, u32[]{:S(2)}, u32[]{:S(2)}) collective-permute-start(bf16[3,256]{1,0:T(4,128)(2,1)S(1)} %slice.433), channel_id=1, source_target_pairs={{0,8},{8,16},{16,24},{24,32},{32,40},{40,48},{48,56},{56,64},{64,7... | collective-permute-start | bytes 4616 | tf_op jit(solution)/shard_map/ppermute | solution.py:18
  43.0 0.8 copy-start.7
  43.5 1.0 copy-start.1
  48.5 39.1 %copy-start.2 = (bf16[384,256]{1,0:T(8,128)(2,1)S(1)}, bf16[384,256]{1,0:T(8,128)(2,1)}, u32[]{:S(2)}) copy-start(bf16[384,256]{1,0:T(8,128)(2,1)} %param.17) | copy-start | bytes 589828
  89.5 39.8 %all-to-all-start = ((bf16[8,48,2048]{2,1,0:T(8,128)(2,1)}), bf16[8,48,2048]{2,1,0:T(8,128)(2,1)S(1)}, u32[]{:S(2)}, u32[]{:S(2)}) async-start(bf16[8,48,2048]{2,1,0:T(8,128)(2,1)} %bitcast.45), calls=%async_computation | async-start | bytes 3145728 | tf_op jit(solution)/shard_map/all_to_all | solution.py:67
  108.7 21.0 %copy-start.3 = (f32[2048]{0:T(1024)S(1)}, f32[2048]{0:T(1024)}, u32[]{:S(2)}) copy-start(f32[2048]{0:T(1024)} %param.24) | copy-start | bytes 24580
  108.7 22.2 %copy-start.4 = (f32[2048]{0:T(1024)S(1)}, f32[2048]{0:T(1024)}, u32[]{:S(2)}) copy-start(f32[2048]{0:T(1024)} %param.25) | copy-start | bytes 24580
  133.4 25.1 %all-to-all-start.1 = ((bf16[8,48,2048]{2,1,0:T(8,128)(2,1)}), bf16[8,48,2048]{2,1,0:T(8,128)(2,1)S(1)}, u32[]{:S(2)}, u32[]{:S(2)}) async-start(bf16[8,48,2048]{2,1,0:T(8,128)(2,1)} %broadcast_in_dim.28), calls=%async_computation.1 | async-start | bytes 3145728 | tf_op jit(solution)/shard_map/all_to_all | solution.py:79
  217.5 0.7 copy-start.5
Sparse Core Ops, SparseCore 0:
  34.9 51.5 all-gather.11
  89.4 85.9 all-gather.9
where the time goes:
time: 228 us; the launch traced here: 227 us
  blocking collectives  95.6 us (42%)
  waiting for transfers between devices  54.4 us (24%)
  starting transfers between devices  26.9 us (12%)
  matrix products  15.7 us (7%)
  between operations  14.3 us (6%)
  local copies, waits for them, and re-layouts  10.4 us (5%)
  other arithmetic  9.44 us (4%)
    all_gather x2, blocking collectives, gathered_once(): both, at, found = (lax.all_gather(jnp.concatenate(lines), axis), 0, {})  38.6 us
    all_to_all x1, blocking collectives, sent_and_summed(): lax.all_to_all(pieces, axis, split_axis=0, concat_axis=0, tiled=True)  28.8 us
    all_gather x1, blocking collectives, stacked_from(): pieces = lax.all_gather(pieces, axes[k])  28.2 us
    all_to_all x1, waiting for transfers between devices, sent_and_summed(): lax.all_to_all(pieces, axis, split_axis=0, concat_axis=0, tiled=True)  20.6 us
    all_to_all x1, starting transfers between devices, sent_and_summed(): lax.all_to_all(pieces, axis, split_axis=0, concat_axis=0, tiled=True)  19.2 us
    all_gather x1, waiting for transfers between devices, sent_together(): lax.all_gather(both, axis, axis=dim, tiled=True)  17 us
    all_to_all x1, waiting for transfers between devices, copy_for_each(): lax.all_to_all(jnp.broadcast_to(value[None], (devices, *value.shape)), ax...  16.8 us
    dot_general x1, matrix products, shards(): jnp.dot(hidden, down_full, preferred_element_type=jnp.float32)  8.56 us
  transfers between devices with their start and end apart: 5, of which 3 were waited for; matrix products, arithmetic and copies ran while one was open for 9% of the time, Pallas kernels for 0%

commit v1 on v0

v1 whole, which is shorter than its diff:
```python
import functools

import jax
import jax.numpy as jnp
from jax import lax
from jax.experimental import pallas as pl
from jax.experimental.pallas import tpu as pltpu
from jax.sharding import PartitionSpec as P

LRU_SCALE = 8.0
NORM_EPS = 1e-06
MESH = pl.DeviceIdType.MESH
F32 = jnp.float32
BF16 = jnp.bfloat16

NF = 8
NX = 4
ROWS = 384
CH = 256
D = 2048
BLK = 48
HID = 704
GL = 1408
WL = 2176
S1A = 1152
NCOPY = 176


def dot(a, b):
    return jnp.dot(a, b, preferred_element_type=F32)


def dot_nt(a, b):
    return lax.dot_general(a, b, (((1,), (1,)), ((), ())), preferred_element_type=F32)


def sigmoid(v):
    return 1.0 / (1.0 + jnp.exp(-v))


def gelu(v):
    inner = 0.7978845608028654 * (v + 0.044715 * (v * v * v))
    return 0.5 * v * (1.0 + jnp.tanh(inner))


def one_minus_exp(w):
    series = 1.0 + w * (1.0 / 6.0)
    for n in (5.0, 4.0, 3.0, 2.0):
        series = 1.0 + w * (1.0 / n) * series
    return jnp.where(w > -0.25, -w * series, 1.0 - jnp.exp(w))


def rms_scale(values, gains):
    mean = jnp.sum(values * values, axis=-1, keepdims=True) * (1.0 / D)
    return values * lax.rsqrt(mean + NORM_EPS) * gains


def kernel(
    resid, x_in, g_in, conv_w, ga_in, gx_in, rate, extra, wp_in, mixg, preg, wg_in, wu_in, wd_in, outg,
    out,
    W, wp, xb, xp, gb, eb, cw, ga, gx, rt, mg, pg, og, wg, wu, wd, rs_b,
    halo, bd, cout, gates, acum, bcum, geb, tot, rowbuf, rtot, colbuf,
    mixa, mixs, mixb, parts, stream,
    sa, s1, s3, rl, rr, fl, fr, nb, hid,
    local_sem, send_sem, recv_sem,
):
    sp = lax.axis_index("sp")
    tp = lax.axis_index("tp")
    z, y = sp // NF, sp % NF
    x, c = tp // 2, tp % 2

    def at_zy(zz, yy):
        return {"sp": zz * NF + yy, "tp": tp}

    def at_x(step):
        return {"sp": sp, "tp": ((x + step) % NX) * 2 + c}

    partner = {"sp": sp, "tp": x * 2 + (1 - c)}
    behind = {"sp": (sp + NF * NF - 1) % (NF * NF), "tp": tp}
    ahead = {"sp": (sp + 1) % (NF * NF), "tp": tp}

    loads = {}

    def load(name, src, dst):
        copy = pltpu.make_async_copy(src, dst, local_sem.at[len(loads)])
        copy.start()
        loads[name] = copy

    load("wg", wg_in, wg)
    load("wu", wu_in, wu)
    load("wd", wd_in, wd)
    load("x", x_in, xb)
    load("ga", ga_in, ga)
    load("gx", gx_in, gx)
    load("g", g_in, gb)
    load("cw", conv_w, cw)
    load("rt", rate, rt)
    load("e", extra, eb)
    load("wp", wp_in, wp.at[0])
    load("rs", resid.at[pl.ds(pl.multiple_of(tp * BLK, 16), BLK), :], rs_b)
    load("mg", mixg, mg)
    load("pg", preg, pg)
    load("og", outg, og)

    barrier = pltpu.get_barrier_semaphore()
    peers = [at_zy(z, (y + k) % NF) for k in range(1, NF)]
    peers += [at_zy((z + k) % NF, y) for k in range(1, NF)]
    peers += [at_x(1), at_x(NX - 1), partner, behind, ahead]
    for peer in peers:
        pl.semaphore_signal(barrier, inc=1, device_id=peer, device_id_type=MESH)

    for name in ("wg", "wu", "wd"):
        loads[name].wait()
    eye = jnp.where(
        lax.broadcasted_iota(jnp.int32, (32, 32), 0) == lax.broadcasted_iota(jnp.int32, (32, 32), 1), 1.0, 0.0
    ).astype(BF16)
    wdt = dot_nt(eye, wd[...]).astype(BF16)
    for h in range(2):
        rows = slice(16 * h, 16 * h + 16)
        mine = W.at[c, z, y, h]
        for n in range(2):
            mine[:, 512 * n : 512 * n + 256] = wg[rows, 256 * n : 256 * n + 256]
            mine[:, 512 * n + 256 : 512 * n + 512] = wu[rows, 256 * n : 256 * n + 256]
        mine[:, 1024:1152] = wg[rows, 512:640]
        mine[:, 1152:1280] = wu[rows, 512:640]
        mine[:, 1280:1408] = jnp.concatenate([wg[rows, 640:704], wu[rows, 640:704]], axis=1)
        mine[:, 1408:2048] = wdt[rows, 0:640]
        mine[:, 2048:2176] = jnp.concatenate([wdt[rows, 640:704], jnp.zeros((16, 64), BF16)], axis=1)

    started = []

    def send(src, dst, device):
        index = len(started)
        copy = pltpu.make_async_remote_copy(
            src_ref=src,
            dst_ref=dst,
            send_sem=send_sem.at[index],
            recv_sem=recv_sem.at[index],
            device_id=device,
            device_id_type=MESH,
        )
        copy.start()
        started.append(copy)
        return copy

    def piece(h, first, second, lanes):
        if h == 0:
            return W.at[c, second, first, 0, :, lanes]
        return W.at[c, first, second, 1, :, lanes]

    def row_of(h, second, lanes, span=slice(0, NF)):
        if h == 0:
            return W.at[c, second, span, 0, :, lanes]
        return W.at[c, span, second, 1, :, lanes]

    first = (y, z)
    second = (z, y)

    def along_first(h, step):
        return at_zy(z, (y + step) % NF) if h == 0 else at_zy((z + step) % NF, y)

    def along_second(h, step):
        return along_first(1 - h, step)

    def mod(v):
        return (v + NF) % NF

    FULL, GLN, DLN = slice(0, WL), slice(0, GL), slice(GL, WL)
    HALVES = (slice(0, 4), slice(4, 8))
    s1c, s2g, s2d, d2d = {}, {}, {}, []

    def hop1(k):
        for h in range(2):
            for d, step in ((0, 1), (1, NF - 1)):
                src = mod(first[h] - (k - 1)) if d == 0 else mod(first[h] + (k - 1))
                lanes = FULL if k < 4 else (slice(0, S1A) if d == 0 else slice(S1A, WL))
                ref = piece(h, src, second[h], lanes)
                s1c[k, h, d] = send(ref, ref, along_first(h, step))

    def hop1_wait(k):
        for h in range(2):
            for d in range(2):
                s1c[k, h, d].wait_recv()

    def spread(js):
        for j in js:
            for h in range(2):
                off = (j + 1) // 2
                src = mod(first[h] - off) if j % 2 == 1 else mod(first[h] + off)
                ref = piece(h, src, second[h], GLN)
                for d, step in ((0, 1), (1, NF - 1)):
                    s2g[1, h, d, j] = send(ref, ref, along_second(h, step))

    def to_partner(h, row, lanes):
        ref = row_of(h, row, lanes)
        d2d.append((lanes, send(ref, ref, partner)))

    def src_row(h, d, t):
        return mod(second[h] - t) if d == 0 else mod(second[h] + t)

    def hop2(table, t, lanes, b):
        for h in range(2):
            for d, step in ((0, 1), (1, NF - 1)):
                if t == 4 and b != d:
                    continue
                ref = row_of(h, src_row(h, d, t - 1), lanes, HALVES[b])
                table[t, h, d, b] = send(ref, ref, along_second(h, step))

    def hop2_wait(table, t, bs):
        for b in bs:
            for h in range(2):
                for d in range(2):
                    if (t, h, d, b) in table:
                        table[t, h, d, b].wait_recv()

    def share(t, lanes):
        for h in range(2):
            for d in range(2 if t < 4 else 1):
                to_partner(h, src_row(h, d, t), lanes)

    loads["x"].wait()
    pl.semaphore_wait(barrier, len(peers))
    halo_copy = send(xb.at[pl.ds(ROWS - 16, 16), :], halo, ahead)
    hop1(1)
    spread([0])
    loads["wp"].wait()
    wp_copy = send(wp.at[0], wp.at[1], partner)

    for name in ("ga", "gx", "g", "cw", "rt", "e"):
        loads[name].wait()
    bd[...] = jnp.zeros_like(bd)
    for n in range(4):
        s = slice(64 * n, 64 * n + 64)
        bd[s, 64 * n : 64 * n + 64] = ga[n]
        bd[s, CH + 64 * n : CH + 64 * n + 64] = gx[n]
    xp[16:, :] = xb[...].astype(F32)
    geb[...] = gelu(gb[...].astype(F32))
    halo_copy.wait_recv()
    xp[0:16, :] = jnp.where(sp > 0, halo[...].astype(F32), 0.0)

    hop1_wait(1)
    hop1(2)
    spread([1, 2])

    conv = xp[13 : 13 + ROWS, :] * cw[0:1, :]
    for tap in range(1, 4):
        conv = conv + xp[13 + tap : 13 + tap + ROWS, :] * cw[tap : tap + 1, :]
    cout[...] = conv.astype(BF16)
    gates[...] = dot(cout[...], bd[...])

    in_group = lax.broadcasted_iota(jnp.int32, (4, 8, CH), 1)

    def chunk(i, carry):
        rows = pl.ds(pl.multiple_of(i * 32, 32), 32)
        recur = sigmoid(gates[rows, 0:CH])
        inject = sigmoid(gates[rows, CH:])
        log_decay = (-LRU_SCALE * recur) * rt[...] + eb[rows, :]
        decay = jnp.exp(log_decay)
        grown = one_minus_exp(2.0 * log_decay)
        root = jnp.where(grown > 0.0, grown * lax.rsqrt(jnp.maximum(grown, 1e-37)), 0.0)
        drive = root * inject * cout[rows, :].astype(F32)
        a = decay.reshape(4, 8, CH)
        b = drive.reshape(4, 8, CH)
        for step in (1, 2, 4):
            keep = in_group >= step
            a_prev = jnp.where(keep, pltpu.roll(a, step, 1), 1.0)
            b_prev = jnp.where(keep, pltpu.roll(b, step, 1), 0.0)
            b = a * b_prev + b
            a = a * a_prev
        a_in, b_in = carry
        a_all, b_all = [], []
        for n in range(4):
            a_n = a[n] * a_in
            b_n = a[n] * b_in + b[n]
            a_in, b_in = a_n[7:8, :], b_n[7:8, :]
            a_all.append(a_n)
            b_all.append(b_n)
        acum[rows, :] = jnp.concatenate(a_all, axis=0)
        bcum[rows, :] = jnp.concatenate(b_all, axis=0)
        return a_in, b_in

    a_end, b_end = lax.fori_loop(0, ROWS // 32, chunk, (jnp.ones((1, CH), F32), jnp.zeros((1, CH), F32)))
    tot[:, 0:CH] = a_end
    tot[:, CH:] = b_end

    row_copies = [send(tot, rowbuf.at[k - 1], at_zy(z, (y + k) % NF)) for k in range(1, NF)]
    hop1_wait(2)
    hop1(3)
    spread([3, 4])
    for copy in row_copies:
        copy.wait_recv()

    def composed(own, buf, me):
        pa, pb = jnp.ones((1, CH), F32), jnp.zeros((1, CH), F32)
        ea, eb_ = pa, pb
        for place in range(NF):
            slot = (me - place + NF) % NF
            got = buf[jnp.maximum(slot - 1, 0)]
            is_me = slot == 0
            va = jnp.where(is_me, own[:, 0:CH], got[:, 0:CH])
            vb = jnp.where(is_me, own[:, CH:], got[:, CH:])
            ea = jnp.where(is_me, pa, ea)
            eb_ = jnp.where(is_me, pb, eb_)
            pa, pb = pa * va, va * pb + vb
        return (pa, pb), (ea, eb_)

    (ra, rb_), (in_a, in_b) = composed(tot[...], rowbuf, y)
    rtot[:, 0:CH] = ra
    rtot[:, CH:] = rb_
    col_copies = [send(rtot, colbuf.at[k - 1], at_zy((z + k) % NF, y)) for k in range(1, NF)]
    hop1_wait(3)
    hop1(4)
    spread([5, 6])
    hop1_wait(4)
    spread([7])
    for h in range(2):
        to_partner(h, second[h], FULL)
    for copy in col_copies:
        copy.wait_recv()
    _, (col_a, col_b) = composed(rtot[...], colbuf, z)
    carried = in_a * col_b + in_b

    def mixer_block(core, rel):
        block = ((x + rel) % NX) * 2 + core
        rows = pl.ds(pl.multiple_of(block * BLK, 16), BLK)
        return ((bcum[rows, :] + acum[rows, :] * carried) * geb[rows, :]).astype(BF16)

    for rel in range(NX):
        mixs[BLK * rel : BLK * rel + BLK, :] = mixer_block(1 - c, rel)
    mix_copy = send(mixs, mixb, partner)
    for rel in range(NX):
        mixa[BLK * rel : BLK * rel + BLK, :] = mixer_block(c, rel)
    parts[...] = dot(mixa[...], wp[0])
    wp_copy.wait_recv()
    mix_copy.wait_recv()
    parts[...] += dot(mixb[...], wp[1])

    def scatter_start(u):
        for half in range(2):
            sa[u, half] = parts[2 * BLK : 3 * BLK, 1024 * half : 1024 * half + 1024].astype(BF16)
        relay_l = send(sa.at[u, 0], rl.at[u], at_x(1))
        relay_r = send(sa.at[u, 1], rr.at[u], at_x(NX - 1))
        s1[u, 1] = parts[BLK : 2 * BLK, 1024:].astype(BF16)
        far_l = send(s1.at[u, 1], fl.at[u, 1], at_x(1))
        s3[u, 0] = parts[3 * BLK :, 0:1024].astype(BF16)
        far_r = send(s3.at[u, 0], fr.at[u, 0], at_x(NX - 1))
        return relay_l, relay_r, far_l, far_r

    def scatter_relay(u, copies):
        relay_l, relay_r = copies[:2]
        relay_l.wait_recv()
        s1[u, 0] = (parts[BLK : 2 * BLK, 0:1024] + rl[u].astype(F32)).astype(BF16)
        near_l = send(s1.at[u, 0], fl.at[u, 0], at_x(1))
        relay_r.wait_recv()
        s3[u, 1] = (parts[3 * BLK :, 1024:] + rr[u].astype(F32)).astype(BF16)
        near_r = send(s3.at[u, 1], fr.at[u, 1], at_x(NX - 1))
        return copies[2:] + (near_l, near_r)

    def scatter_end(u, copies):
        for copy in copies:
            copy.wait_recv()
        halves = [
            parts[0:BLK, 1024 * half : 1024 * half + 1024] + fl[u, half].astype(F32) + fr[u, half].astype(F32)
            for half in range(2)
        ]
        return jnp.concatenate(halves, axis=1)

    copies = scatter_start(0)
    hop2_wait_list = [s2g[1, h, d, j] for j in range(NF) for h in range(2) for d in range(2)]
    for copy in hop2_wait_list:
        copy.wait_recv()
    hop2(s2g, 2, GLN, 0)
    copies = scatter_relay(0, copies)
    hop2(s2g, 2, GLN, 1)
    share(1, GLN)
    for name in ("rs", "mg", "pg", "og"):
        loads[name].wait()
    hop2_wait(s2g, 2, (0,))
    hop2(s2g, 3, GLN, 0)
    mixed = scatter_end(0, copies)
    after_mix = rs_b[...].astype(F32) + rms_scale(mixed, mg[...])
    stream[...] = after_mix
    normed = rms_scale(after_mix, pg[...]).astype(BF16)
    nb[0, 0] = normed[:, 0:1024]
    nb[1, 0] = normed[:, 1024:]

    left_a = send(nb.at[0, 0], nb.at[0, 3], at_x(1))
    right_a = send(nb.at[1, 0], nb.at[1, 1], at_x(NX - 1))
    left_b = send(nb.at[1, 0], nb.at[1, 3], at_x(1))
    right_b = send(nb.at[0, 0], nb.at[0, 1], at_x(NX - 1))
    hop2_wait(s2g, 2, (1,))
    hop2(s2g, 3, GLN, 1)
    share(2, GLN)
    left_a.wait_recv()
    left_c = send(nb.at[0, 3], nb.at[0, 2], at_x(1))
    right_a.wait_recv()
    right_c = send(nb.at[1, 1], nb.at[1, 2], at_x(NX - 1))
    hop2_wait(s2g, 3, (0, 1))
    hop2(s2g, 4, GLN, 0)
    hop2(s2g, 4, GLN, 1)
    share(3, GLN)
    for b in range(2):
        for h in range(2):
            for d, step in ((0, 1), (1, NF - 1)):
                ref = row_of(h, second[h], DLN, HALVES[b])
                s2d[1, h, d, b] = send(ref, ref, along_second(h, step))
    for copy in (left_b, right_b, left_c, right_c):
        copy.wait_recv()
    hop2_wait(s2g, 4, (0, 1))
    share(4, GLN)
    for lanes, copy in d2d:
        copy.wait_recv()
    n_shared = len(d2d)

    def gate_up(core, lanes):
        w = W[core, :, :, :, :, lanes]
        w = w.reshape(D, w.shape[-1])
        acc = dot(nb[0].reshape(NX * BLK, 1024), w[0:1024])
        return acc + dot(nb[1].reshape(NX * BLK, 1024), w[1024:])

    for core in range(2):
        for n in range(2):
            both = gate_up(core, slice(512 * n, 512 * n + 512))
            g, u = both[:, 0:256], both[:, 256:512]
            hid[core, :, 256 * n : 256 * n + 256] = (g * sigmoid(g) * u).astype(BF16)
        both = gate_up(core, slice(1024, 1408))
        g, u = both[:, 0:128], both[:, 128:256]
        hid[core, :, 512:640] = (g * sigmoid(g) * u).astype(BF16)
        last = both[:, 256:384]
        g, u = last, pltpu.roll(last, 64, 1)
        lane = lax.broadcasted_iota(jnp.int32, last.shape, 1)
        hid[core, :, 640:768] = jnp.where(lane < 64, g * sigmoid(g) * u, 0.0).astype(BF16)
        if core == 0:
            hop2_wait(s2d, 1, (0,))
            hop2(s2d, 2, DLN, 0)
            hop2_wait(s2d, 1, (1,))
            hop2(s2d, 2, DLN, 1)
            share(1, DLN)
    hop2_wait(s2d, 2, (0,))
    hop2(s2d, 3, DLN, 0)
    hop2_wait(s2d, 2, (1,))
    hop2(s2d, 3, DLN, 1)
    share(2, DLN)
    hop2_wait(s2d, 3, (0, 1))
    hop2(s2d, 4, DLN, 0)
    hop2(s2d, 4, DLN, 1)
    share(3, DLN)
    hop2_wait(s2d, 4, (0, 1))
    share(4, DLN)
    for lanes, copy in d2d[n_shared:]:
        copy.wait_recv()

    def down(n, _):
        acc = jnp.zeros((NX * BLK, 256), F32)
        for core in range(2):
            w = W[core, n, :, :, :, slice(GL, WL)]
            acc = acc + dot_nt(hid[core], w.reshape(256, WL - GL))
        parts[:, pl.ds(pl.multiple_of(n * 256, 256), 256)] = acc
        return 0

    lax.fori_loop(0, NF, down, 0)
    copies = scatter_start(1)
    copies = scatter_relay(1, copies)
    ffn = scatter_end(1, copies)
    out[...] = (stream[...] + 0.5 * rms_scale(ffn, og[...])).astype(BF16)
    for copy in started:
        copy.wait_send()


def shards(
    resid, x_branch, gate_branch, conv_w, gate_a_w, gate_x_w, decay_rate, decay_extra, w_proj, mix_gain,
    pre_gain, w_gate, w_up, w_down, out_gain,
):
    vmem = pltpu.VMEM
    half = (2, BLK, 1024)
    return pl.pallas_call(
        kernel,
        out_shape=jax.ShapeDtypeStruct((BLK, D), BF16),
        in_specs=[pl.BlockSpec(memory_space=pl.ANY)] * 15,
        out_specs=pl.BlockSpec(memory_space=pltpu.VMEM),
        scratch_shapes=[
            vmem((2, NF, NF, 2, 16, WL), BF16),
            vmem((2, CH, D), BF16),
            vmem((ROWS, CH), BF16),
            vmem((ROWS + 16, CH), F32),
            vmem((ROWS, CH), BF16),
            vmem((ROWS, CH), F32),
            vmem((4, CH), F32),
            vmem((4, 64, 64), BF16),
            vmem((4, 64, 64), BF16),
            vmem((1, CH), F32),
            vmem((1, D), F32),
            vmem((1, D), F32),
            vmem((1, D), F32),
            vmem((32, HID), BF16),
            vmem((32, HID), BF16),
            vmem((HID, 32), BF16),
            vmem((BLK, D), BF16),
            vmem((16, CH), BF16),
            vmem((CH, 2 * CH), BF16),
            vmem((ROWS, CH), BF16),
            vmem((ROWS, 2 * CH), F32),
            vmem((ROWS, CH), F32),
            vmem((ROWS, CH), F32),
            vmem((ROWS, CH), F32),
            vmem((1, 2 * CH), F32),
            vmem((NF - 1, 1, 2 * CH), F32),
            vmem((1, 2 * CH), F32),
            vmem((NF - 1, 1, 2 * CH), F32),
            vmem((NX * BLK, CH), BF16),
            vmem((NX * BLK, CH), BF16),
            vmem((NX * BLK, CH), BF16),
            vmem((NX * BLK, D), F32),
            vmem((BLK, D), F32),
            vmem((2,) + half, BF16),
            vmem((2,) + half, BF16),
            vmem((2,) + half, BF16),
            vmem(half, BF16),
            vmem(half, BF16),
            vmem((2,) + half, BF16),
            vmem((2,) + half, BF16),
            vmem((2, NX, BLK, 1024), BF16),
            vmem((2, NX * BLK, 768), BF16),
            pltpu.SemaphoreType.DMA((15,)),
            pltpu.SemaphoreType.DMA((NCOPY,)),
            pltpu.SemaphoreType.DMA((NCOPY,)),
        ],
        compiler_params=pltpu.CompilerParams(
            collective_id=0, has_side_effects=True, vmem_limit_bytes=58 * 1024 * 1024
        ),
        name="layer",
    )(
        resid, x_branch, gate_branch, conv_w, gate_a_w, gate_x_w, decay_rate.reshape(1, CH), decay_extra,
        w_proj, mix_gain.reshape(1, D), pre_gain.reshape(1, D), w_gate, w_up, w_down, out_gain.reshape(1, D),
    )


def solution(mesh):
    return jax.shard_map(
        shards,
        mesh=mesh,
        in_specs=(
            P("sp", None),
            P("sp", "tp"),
            P("sp", "tp"),
            P(None, "tp"),
            P("tp", None, None),
            P("tp", None, None),
            P("tp"),
            P("sp", "tp"),
            P("tp", None),
            P(),
            P(),
            P("sp", "tp"),
            P("sp", "tp"),
            P("tp", "sp"),
            P(),
        ),
        out_specs=P(("sp", "tp"), None),
        check_vma=False,
    )
```

time: 228 us -> 101 us (0.44)
  Pallas kernels: 0 us -> 97.2 us
  blocking collectives: 95.6 us -> 0 us
  waiting for transfers between devices: 54.4 us -> 0 us
  starting transfers between devices: 26.9 us -> 0 us
  matrix products: 15.7 us -> 0 us
  between operations: 14.3 us -> 0.01 us
  other arithmetic: 9.44 us -> 0 us
  local copies, waits for them, and re-layouts: 10.4 us -> 3.22 us
    pallas_call x0 -> x1, Pallas kernels: none -> 97.2 us  [shards(): pl.pallas_call(kernel, out_shape=jax.ShapeDtypeStruct((BLK, D), BF16), in...]
    all_gather x3 -> x0, blocking collectives: 66.8 us -> none  [the longest x2 38.6 us: gathered_once(): both, at, found = (lax.all_gather(jnp.concatenate(lines), axis), 0, {})]
    all_to_all x2 -> x0, waiting for transfers between devices: 37.4 us -> none  [the longest x1 20.6 us: sent_and_summed(): lax.all_to_all(pieces, axis, split_axis=0, concat_axis=0, tiled=True)]
    all_to_all x1 -> x0, blocking collectives: 28.8 us -> none  [sent_and_summed(): lax.all_to_all(pieces, axis, split_axis=0, concat_axis=0, tiled=True)]
    all_to_all x2 -> x0, starting transfers between devices: 23.7 us -> none  [the longest x1 19.2 us: sent_and_summed(): lax.all_to_all(pieces, axis, split_axis=0, concat_axis=0, tiled=True)]
    all_gather x2 -> x0, waiting for transfers between devices: 17 us -> none  [the longest x1 17 us: sent_together(): lax.all_gather(both, axis, axis=dim, tiled=True)]
    dot_general x5 -> x0, matrix products: 15.7 us -> none  [the longest x1 8.56 us: shards(): jnp.dot(hidden, down_full, preferred_element_type=jnp.float32)]
    convert_element_type x4 -> x0, other arithmetic: 4.03 us -> none  [the longest x1 1.79 us: shards(): return (after_mix + 0.5 * rms_scale(ffn, out_gain)).astype(jnp.bfloat16)]
  transfers between devices with their start and end apart: 5 -> 0, of which waited for: 3 -> 0; matrix products, arithmetic and copies ran while one was open for 9% -> 0% of each run, Pallas kernels for 0% -> 0%
where the time goes in v1:
time: 101 us; the launch traced here: 100 us
  Pallas kernels  97.2 us (96%)
  local copies, waits for them, and re-layouts  3.22 us (3%)
    pallas_call x1, Pallas kernels, shards(): pl.pallas_call(kernel, out_shape=jax.ShapeDtypeStruct((BLK, D), BF16), in...  97.2 us
    unnamed x2, local copies, waits for them, and re-layouts  3.22 us

profile of v1, /device:TPU:1, one launch (start us, length us, event | category | flops | bytes accessed | tf_op | source)
XLA Modules:
  0.0 100.5 jit_solution(3666889219939920873)
XLA Ops:
  0.0 1.6 %copy.16.wd_in = bf16[704,32]{1,0:T(8,128)(2,1)} copy(bf16[704,32]{0,1:T(8,128)(2,1)} %param.28) | data formatting | bytes 90112 | tf_op args[13]
  1.6 97.2 %layer.1 = bf16[48,2048]{1,0:T(8,128)(2,1)} custom-call(bf16[384,2048]{1,0:T(8,128)(2,1)} %resid.1, bf16[384,256]{1,0:T(8,128)(2,1)} %x_in.1, bf16[384,256]{1,0:T(8,128)(2,1)} %g_in.1, f32[4,256]{1,0:T(4,128)} %conv_w.1, bf16[4,64,64]{2,1,0:T(8,128)(2,1)} %ga_in.1, bf16[4,64,64]{2,1,0:T(8,128)(2,1)} %gx_in.1, f32[1,256]{1,0:T(1,128)} %bitcast.7, ...), custom_call_target="tpu_custom_call" | custom-call | tf_op jit(solution)/shard_map/layer/pallas_call | solution.py:476
  98.8 1.6 %copy.18 = bf16[48,2048]{1,0:T(8,128)(2,1)} copy(bf16[48,2048]{1,0:T(8,128)(2,1)} %layer.1) | data formatting | bytes 393216

commit v2 on v1

v2 whole, which is shorter than its diff:
```python
import functools

import jax
import jax.numpy as jnp
from jax import lax
from jax.experimental import pallas as pl
from jax.experimental.pallas import tpu as pltpu
from jax.sharding import PartitionSpec as P

LRU_SCALE = 8.0
NORM_EPS = 1e-06
MESH = pl.DeviceIdType.MESH
F32 = jnp.float32
BF16 = jnp.bfloat16

NF = 8
NX = 4
ROWS = 384
CH = 256
D = 2048
BLK = 48
HID = 704
WL = 2176
DA, GA, GB, DB = slice(0, 512), slice(512, 1152), slice(1152, 1920), slice(1920, 2176)
LA, LB, GU, ALL = slice(0, 1152), slice(1152, WL), slice(512, 1920), slice(0, WL)
LANES = {"DA": DA, "GA": GA, "GB": GB, "DB": DB}
GROUPS = ((0,), (1, 2), (3, 4), (5, 6), (7,))
NRECV = 110
NSEND = 22

ORDER = (
    ("DA", 0, 0), ("DB", 0, 0), ("scan", 0, 0), ("SB", 1, 0), ("SA", 1, 0), ("GA", 1, 0), ("GB", 1, 0),
    ("DA", 1, 0), ("DB", 1, 0), ("SB", 2, 0), ("GB", 1, 1), ("row", 0, 0), ("GA", 1, 1), ("SA", 2, 0),
    ("GA", 2, 0), ("DA", 2, 0), ("GB", 2, 0), ("DB", 2, 0), ("SB", 3, 0), ("GB", 1, 2), ("GA", 2, 1),
    ("col", 0, 0), ("mix", 0, 0), ("GB", 2, 1), ("GA", 1, 2), ("GA", 3, 0), ("SA", 3, 0), ("DA", 3, 0),
    ("mix2", 0, 0), ("GB", 3, 0), ("SB", 4, 0), ("DB", 3, 0), ("GA", 3, 1), ("GB", 1, 3), ("GA", 2, 2),
    ("relay", 0, 0), ("GA", 4, 0), ("GB", 2, 2), ("GA", 1, 3), ("DA", 4, 0), ("GB", 3, 1), ("GA", 4, 1),
    ("SA", 4, 0), ("send", 0, 0), ("GB", 4, 0), ("GA", 3, 2), ("GB", 1, 4), ("PGB", 1, 0), ("DB", 4, 0),
    ("DA", 0, 1), ("GA", 2, 3), ("GB", 2, 3), ("GA", 1, 4), ("PGA", 1, 0), ("GA", 4, 2), ("ag", 0, 0),
    ("GB", 3, 2), ("DA", 1, 1), ("GB", 4, 1), ("DA", 0, 2), ("GA", 3, 3), ("GB", 2, 4), ("PGB", 2, 0),
    ("GA", 2, 4), ("PGA", 2, 0), ("agend", 0, 0), ("DB", 0, 1), ("GB", 3, 3), ("DA", 2, 1), ("GB", 4, 2),
    ("DB", 0, 2), ("DA", 1, 2), ("DB", 0, 3), ("GB", 3, 4), ("PGB", 3, 0), ("GA", 4, 3), ("DB", 1, 1),
    ("GA", 3, 4), ("PGA", 3, 0), ("GB", 4, 3), ("DA", 0, 3), ("DB", 0, 4), ("DB", 1, 2), ("DA", 3, 1),
    ("DB", 1, 3), ("GB", 4, 4), ("PGB", 4, 0), ("DA", 0, 4), ("DA", 2, 2), ("GA", 4, 4), ("PGA", 4, 0),
    ("DB", 2, 1), ("DB", 1, 4), ("PDB", 1, 0), ("DB", 2, 2), ("DA", 1, 3), ("gw", 0, 0), ("gu0", 0, 0),
    ("DB", 2, 3), ("gu1", 0, 0), ("DA", 4, 1), ("gu2", 0, 0), ("DB", 3, 1), ("DA", 1, 4), ("PDA", 1, 0),
    ("DB", 2, 4), ("PDB", 2, 0), ("gu3", 0, 0), ("DB", 3, 2), ("gu4", 0, 0), ("DA", 3, 2), ("DB", 3, 3),
    ("gu5", 0, 0), ("DA", 2, 3), ("DB", 4, 1), ("DB", 3, 4), ("PDB", 3, 0), ("DA", 2, 4), ("PDA", 2, 0),
    ("DB", 4, 2), ("DB", 4, 3), ("DA", 4, 2), ("DB", 4, 4), ("PDB", 4, 0), ("DA", 3, 3), ("g0", 0, 0),
    ("DA", 3, 4), ("PDA", 3, 0), ("DA", 4, 3), ("g1", 0, 0), ("DA", 4, 4), ("PDA", 4, 0), ("g2", 0, 0),
    ("g0r", 0, 0),
)


def dot(a, b):
    return jnp.dot(a, b, preferred_element_type=F32)


def dot_nt(a, b):
    return lax.dot_general(a, b, (((1,), (1,)), ((), ())), preferred_element_type=F32)


def sigmoid(v):
    return 1.0 / (1.0 + jnp.exp(-v))


def gelu(v):
    inner = 0.7978845608028654 * (v + 0.044715 * (v * v * v))
    return 0.5 * v * (1.0 + jnp.tanh(inner))


def one_minus_exp(w):
    series = 1.0 + w * (1.0 / 6.0)
    for n in (5.0, 4.0, 3.0, 2.0):
        series = 1.0 + w * (1.0 / n) * series
    return jnp.where(w > -0.25, -w * series, 1.0 - jnp.exp(w))


def rms_scale(values, gains):
    mean = jnp.sum(values * values, axis=-1, keepdims=True) * (1.0 / D)
    return values * lax.rsqrt(mean + NORM_EPS) * gains


def kernel(
    resid, x_in, g_in, conv_w, ga_in, gx_in, rate, extra, wp_in, mixg, preg, wg_in, wu_in, wd_in, outg,
    out,
    W, wp, xb, xp, gb, eb, cw, ga, gx, rt, mg, pg, og, wg, wu, wd, rs_b,
    halo, bd, cout, gates, acum, bcum, geb, tot, rowbuf, rtot, colbuf,
    mixa, mixs, mixb, parts, stream, sb, rl, rr, fl, fr, nb, hid,
    parts2, sb0, rl0, rr0, fl0, fr0, sb1, rb1, sb2, rb2, ffn,
    local_sem, send_sem, recv_sem,
):
    sp = lax.axis_index("sp")
    tp = lax.axis_index("tp")
    z, y = sp // NF, sp % NF
    x, c = tp // 2, tp % 2

    def at_zy(zz, yy):
        return {"sp": zz * NF + yy, "tp": tp}

    def at_x(step):
        return {"sp": sp, "tp": ((x + step) % NX) * 2 + c}

    partner = {"sp": sp, "tp": x * 2 + (1 - c)}
    behind = {"sp": (sp + NF * NF - 1) % (NF * NF), "tp": tp}
    ahead = {"sp": (sp + 1) % (NF * NF), "tp": tp}

    loads = {}

    def load(name, src, dst):
        copy = pltpu.make_async_copy(src, dst, local_sem.at[len(loads)])
        copy.start()
        loads[name] = copy

    load("wg", wg_in, wg)
    load("wu", wu_in, wu)
    load("wd", wd_in, wd)
    load("x", x_in, xb)
    load("ga", ga_in, ga)
    load("gx", gx_in, gx)
    load("g", g_in, gb)
    load("cw", conv_w, cw)
    load("rt", rate, rt)
    load("e", extra, eb)
    load("wp", wp_in, wp.at[0])
    load("rs", resid.at[pl.ds(pl.multiple_of(tp * BLK, 16), BLK), :], rs_b)
    load("mg", mixg, mg)
    load("pg", preg, pg)
    load("og", outg, og)

    barrier = pltpu.get_barrier_semaphore()
    peers = [at_zy(z, (y + k) % NF) for k in range(1, NF)]
    peers += [at_zy((z + k) % NF, y) for k in range(1, NF)]
    peers += [at_x(1), at_x(2), at_x(NX - 1), partner, behind, ahead]
    for peer in peers:
        pl.semaphore_signal(barrier, inc=1, device_id=peer, device_id_type=MESH)

    for name in ("wg", "wu", "wd"):
        loads[name].wait()
    mine = W.at[c, z, y]
    mine[:, 0:512] = wd[:, 0:512]
    for n in range(2):
        mine[:, 512 * n + 512 : 512 * n + 768] = wg[:, 256 * n : 256 * n + 256]
        mine[:, 512 * n + 768 : 512 * n + 1024] = wu[:, 256 * n : 256 * n + 256]
    mine[:, 1536:1664] = wg[:, 512:640]
    mine[:, 1664:1792] = wu[:, 512:640]
    mine[:, 1792:1920] = jnp.concatenate([wg[:, 640:704], wu[:, 640:704]], axis=1)
    mine[:, 1920:2048] = wd[:, 512:640]
    mine[:, 2048:2176] = jnp.concatenate([wd[:, 640:704], jnp.zeros((32, 64), BF16)], axis=1)

    send_ids, recv_ids = {}, {}

    def send(src, dst, device, to, out):
        copy = pltpu.make_async_remote_copy(
            src_ref=src,
            dst_ref=dst,
            send_sem=send_sem.at[send_ids.setdefault(out, len(send_ids))],
            recv_sem=recv_sem.at[recv_ids.setdefault(to, len(recv_ids))],
            device_id=device,
            device_id_type=MESH,
        )
        copy.start()

    def arrived(to, like):
        pltpu.make_async_copy(like, like, recv_sem.at[recv_ids[to]]).wait()

    def sent(out, like):
        pltpu.make_async_copy(like, like, send_sem.at[send_ids[out]]).wait()

    def mod(v):
        return (v + NF) % NF

    def piece(fam, first, second, lanes):
        return W.at[c, second, first, :, lanes] if fam == "A" else W.at[c, first, second, :, lanes]

    def row_of(fam, second, lanes):
        return W.at[c, second, :, :, lanes] if fam == "A" else W.at[c, :, second, :, lanes]

    def some(n, lanes):
        return W.at[c, 0, 0:n, :, lanes]

    first = {"A": y, "B": z}
    second = {"A": z, "B": y}

    def along_y(step):
        return at_zy(z, (y + step) % NF)

    def along_z(step):
        return at_zy((z + step) % NF, y)

    along_first = {"A": along_y, "B": along_z}
    along_second = {"A": along_z, "B": along_y}
    WAYS = ((1, -1), (NF - 1, 1))

    def hop1(fam, k):
        whole = LA if fam == "A" else LB
        cut = whole.start + (640 if fam == "A" else 512)
        for d, (step, sign) in enumerate(WAYS):
            lanes = whole if k < 4 else (slice(whole.start, cut) if d == 0 else slice(cut, whole.stop))
            ref = piece(fam, mod(first[fam] + sign * (k - 1)), second[fam], lanes)
            send(ref, ref, along_first[fam](step), ("S" + fam, k), "S" + fam)

    def hop1_done(fam, k):
        whole = LA if fam == "A" else LB
        arrived(("S" + fam, k), some(2 if k < 4 else 1, whole))

    def offset(j):
        return (j + 1) // 2 * (-1 if j % 2 == 1 else 1)

    def hop2(name, t, q):
        fam, lanes = name[1], LANES[name]
        for d, (step, sign) in enumerate(WAYS):
            for j in GROUPS[q]:
                if t == 4 and (j < 4) != (d == 0):
                    continue
                ref = piece(fam, mod(first[fam] + offset(j)), mod(second[fam] + sign * (t - 1)), lanes)
                send(ref, ref, along_second[fam](step), (name, t, q), name)

    def hop2_done(name, t, q):
        n = len(GROUPS[q])
        arrived((name, t, q), some(2 * n if t < 4 else n, LANES[name]))

    def to_partner(name, t):
        fam = name[1]
        for sign in (-1, 1)[: 2 if t < 4 else 1]:
            ref = row_of(fam, mod(second[fam] + sign * t), LANES[name])
            to = "PG" if name[0] == "G" else ("PDB" if fam == "B" else ("PDA", max(t, 2)))
            send(ref, ref, partner, to, to)

    loads["x"].wait()
    pl.semaphore_wait(barrier, len(peers))
    hop1("A", 1)
    hop1("B", 1)
    send(xb.at[pl.ds(ROWS - 16, 16), :], halo, ahead, "halo", "halo")
    hop2("GA", 1, 0)
    hop2("GB", 1, 0)
    loads["wp"].wait()
    send(wp.at[0], wp.at[1], partner, "wp", "wp")
    for name in ("ga", "gx", "g", "cw", "rt", "e"):
        loads[name].wait()
    bd[...] = jnp.zeros_like(bd)
    for n in range(4):
        s = slice(64 * n, 64 * n + 64)
        bd[s, 64 * n : 64 * n + 64] = ga[n]
        bd[s, CH + 64 * n : CH + 64 * n + 64] = gx[n]
    xp[16:, :] = xb[...].astype(F32)
    geb[...] = gelu(gb[...].astype(F32))

    def scan():
        arrived("halo", halo)
        xp[0:16, :] = jnp.where(sp > 0, halo[...].astype(F32), 0.0)
        conv = xp[13 : 13 + ROWS, :] * cw[0:1, :]
        for tap in range(1, 4):
            conv = conv + xp[13 + tap : 13 + tap + ROWS, :] * cw[tap : tap + 1, :]
        cout[...] = conv.astype(BF16)
        gates[...] = dot(cout[...], bd[...])
        in_group = lax.broadcasted_iota(jnp.int32, (4, 8, CH), 1)

        def chunk(i, carry):
            rows = pl.ds(pl.multiple_of(i * 32, 32), 32)
            recur = sigmoid(gates[rows, 0:CH])
            inject = sigmoid(gates[rows, CH:])
            log_decay = (-LRU_SCALE * recur) * rt[...] + eb[rows, :]
            decay = jnp.exp(log_decay)
            grown = one_minus_exp(2.0 * log_decay)
            root = jnp.where(grown > 0.0, grown * lax.rsqrt(jnp.maximum(grown, 1e-37)), 0.0)
            drive = root * inject * cout[rows, :].astype(F32)
            a = decay.reshape(4, 8, CH)
            b = drive.reshape(4, 8, CH)
            for step in (1, 2, 4):
                keep = in_group >= step
                a_prev = jnp.where(keep, pltpu.roll(a, step, 1), 1.0)
                b_prev = jnp.where(keep, pltpu.roll(b, step, 1), 0.0)
                b = a * b_prev + b
                a = a * a_prev
            a_in, b_in = carry
            a_all, b_all = [], []
            for n in range(4):
                a_n = a[n] * a_in
                b_n = a[n] * b_in + b[n]
                a_in, b_in = a_n[7:8, :], b_n[7:8, :]
                a_all.append(a_n)
                b_all.append(b_n)
            acum[rows, :] = jnp.concatenate(a_all, axis=0)
            bcum[rows, :] = jnp.concatenate(b_all, axis=0)
            return a_in, b_in

        start = (jnp.ones((1, CH), F32), jnp.zeros((1, CH), F32))
        a_end, b_end = lax.fori_loop(0, ROWS // 32, chunk, start)
        tot[:, 0:CH] = a_end
        tot[:, CH:] = b_end
        for k in range(1, NF):
            send(tot, rowbuf.at[k - 1], along_y(k), "row", "row")

    def composed(own, buf, me):
        pa, pb = jnp.ones((1, CH), F32), jnp.zeros((1, CH), F32)
        ea, eb_ = pa, pb
        for place in range(NF):
            slot = (me - place + NF) % NF
            got = buf[jnp.maximum(slot - 1, 0)]
            is_me = slot == 0
            va = jnp.where(is_me, own[:, 0:CH], got[:, 0:CH])
            vb = jnp.where(is_me, own[:, CH:], got[:, CH:])
            ea = jnp.where(is_me, pa, ea)
            eb_ = jnp.where(is_me, pb, eb_)
            pa, pb = pa * va, va * pb + vb
        return (pa, pb), (ea, eb_)

    held = {}

    def row():
        arrived("row", rowbuf)
        (ra, rb_), held["in"] = composed(tot[...], rowbuf, y)
        rtot[:, 0:CH] = ra
        rtot[:, CH:] = rb_
        for k in range(1, NF):
            send(rtot, colbuf.at[k - 1], along_z(k), "col", "col")

    def col():
        arrived("col", colbuf)
        _, (col_a, col_b) = composed(rtot[...], colbuf, z)
        in_a, in_b = held["in"]
        held["carried"] = in_a * col_b + in_b

    def mixer_block(core, rel):
        block = ((x + rel) % NX) * 2 + core
        rows = pl.ds(pl.multiple_of(block * BLK, 16), BLK)
        return ((bcum[rows, :] + acum[rows, :] * held["carried"]) * geb[rows, :]).astype(BF16)

    def mix():
        for rel in range(NX):
            mixs[BLK * rel : BLK * rel + BLK, :] = mixer_block(1 - c, rel)
        send(mixs, mixb, partner, "mix", "mix")
        for rel in range(NX):
            mixa[BLK * rel : BLK * rel + BLK, :] = mixer_block(c, rel)
        arrived("wp", wp.at[1])
        parts[...] = dot(mixa[...], wp[0])

    def scatter_start(u, take, sbuf, bufs):
        rl_, rr_, fl_, fr_ = bufs
        for half in range(2):
            sbuf[half] = take(2, half).astype(BF16)
        send(sbuf.at[0], rl_, at_x(1), ("rl", u), ("sb", u))
        send(sbuf.at[1], rr_, at_x(NX - 1), ("rr", u), ("sb", u))
        sbuf[2] = take(1, 1).astype(BF16)
        send(sbuf.at[2], fl_.at[1], at_x(1), ("f", u), ("sb", u))
        sbuf[3] = take(3, 0).astype(BF16)
        send(sbuf.at[3], fr_.at[0], at_x(NX - 1), ("f", u), ("sb", u))

    def scatter_relay(u, take, sbuf, bufs):
        rl_, rr_, fl_, fr_ = bufs
        arrived(("rl", u), rl_)
        sbuf[4] = (take(1, 0) + rl_[...].astype(F32)).astype(BF16)
        send(sbuf.at[4], fl_.at[0], at_x(1), ("f", u), ("sb", u))
        arrived(("rr", u), rr_)
        sbuf[5] = (take(3, 1) + rr_[...].astype(F32)).astype(BF16)
        send(sbuf.at[5], fr_.at[1], at_x(NX - 1), ("f", u), ("sb", u))

    bufs = (rl, rr, fl, fr)

    def take(rel, half):
        return parts[BLK * rel : BLK * rel + BLK, 1024 * half : 1024 * half + 1024]

    def mix2():
        arrived("mix", mixb)
        parts[...] += dot(mixb[...], wp[1])
        scatter_start(0, take, sb, bufs)

    def relay():
        scatter_relay(0, take, sb, bufs)

    def norm_and_send():
        arrived(("f", 0), sb.at[0:4])
        for name in ("rs", "mg", "pg", "og"):
            loads[name].wait()
        halves = [take(0, half) + fl[half].astype(F32) + fr[half].astype(F32) for half in range(2)]
        mixed = jnp.concatenate(halves, axis=1)
        after_mix = rs_b[...].astype(F32) + rms_scale(mixed, mg[...])
        stream[...] = after_mix
        normed = rms_scale(after_mix, pg[...]).astype(BF16)
        nb[0, 0] = normed[:, 0:1024]
        nb[1, 0] = normed[:, 1024:]
        send(nb.at[0, 0], nb.at[0, 3], at_x(1), "al", "nb")
        send(nb.at[1, 0], nb.at[1, 1], at_x(NX - 1), "ar", "nb")
        send(nb.at[1, 0], nb.at[1, 3], at_x(1), "ab", "nb")
        send(nb.at[0, 0], nb.at[0, 1], at_x(NX - 1), "ab", "nb")

    def ag():
        arrived("al", nb.at[0, 3])
        send(nb.at[0, 3], nb.at[0, 2], at_x(1), "ab", "nb")
        arrived("ar", nb.at[1, 1])
        send(nb.at[1, 1], nb.at[1, 2], at_x(NX - 1), "ab", "nb")

    def agend():
        arrived("ab", nb.at[0])

    def gw():
        arrived("P0", W.at[c, 0, :, :, ALL])
        arrived("PG", W.at[c, 0:7, :, :, GU])

    def gate_up(core, lanes):
        w = W[core, :, :, :, lanes]
        w = w.reshape(D, w.shape[-1])
        acc = dot(nb[0].reshape(NX * BLK, 1024), w[0:1024])
        return acc + dot(nb[1].reshape(NX * BLK, 1024), w[1024:])

    def gu(i):
        core, n = i // 3, i % 3
        if n < 2:
            both = gate_up(core, slice(512 * n + 512, 512 * n + 1024))
            g, u = both[:, 0:256], both[:, 256:512]
            hid[core, :, 256 * n : 256 * n + 256] = (g * sigmoid(g) * u).astype(BF16)
        else:
            both = gate_up(core, slice(1536, 1920))
            g, u = both[:, 0:128], both[:, 128:256]
            hid[core, :, 512:640] = (g * sigmoid(g) * u).astype(BF16)
            g = both[:, 256:384]
            u = pltpu.roll(g, 64, 1)
            lane = lax.broadcasted_iota(jnp.int32, g.shape, 1)
            hid[core, :, 640:768] = jnp.where(lane < 64, g * sigmoid(g) * u, 0.0).astype(BF16)

    def place(i):
        return (z + NF + (i + 1) // 2 * (1 - 2 * (i % 2))) % NF

    def down(i, _):
        acc = jnp.zeros((NX * BLK, 256), F32)
        for core in range(2):
            wa = W[core, place(i), :, :, DA].reshape(256, 512)
            wb = W[core, place(i), :, :, DB].reshape(256, 256)
            acc = acc + dot_nt(hid[core, :, 0:512], wa) + dot_nt(hid[core, :, 512:768], wb)
        parts2[i] = acc
        return 0

    bufs0 = (rl0, rr0, fl0, fr0)

    def take0(rel, half):
        return parts2[0:5, BLK * rel : BLK * rel + BLK, 128 * half : 128 * half + 128]

    def g0():
        arrived("PDB", W.at[c, 0:7, :, :, DB])
        arrived(("PDA", 2), W.at[c, 0:4, :, :, DA])
        lax.fori_loop(0, 5, down, 0)
        scatter_start(1, take0, sb0, bufs0)

    def g0r():
        scatter_relay(1, take0, sb0, bufs0)

    def direct(u, lo, hi, sbuf, rbuf):
        for k, (rel, step) in enumerate(((2, 2), (1, 1), (3, NX - 1))):
            sbuf[k] = parts2[lo:hi, BLK * rel : BLK * rel + BLK, :].astype(BF16)
            send(sbuf.at[k], rbuf.at[k], at_x(step), ("d", u), ("d", u))

    def g1():
        arrived(("PDA", 3), W.at[c, 0:2, :, :, DA])
        lax.fori_loop(5, 7, down, 0)
        direct(1, 5, 7, sb1, rb1)

    def g2():
        arrived(("PDA", 4), W.at[c, 0, :, :, DA])
        down(7, 0)
        direct(2, 7, 8, sb2, rb2)

    steps = {
        "scan": scan, "row": row, "col": col, "mix": mix, "mix2": mix2, "relay": relay, "send": norm_and_send,
        "ag": ag, "agend": agend, "gw": gw, "g0": g0, "g0r": g0r, "g1": g1, "g2": g2,
    }
    for i in range(6):
        steps["gu%d" % i] = functools.partial(gu, i)

    for name, t, q in ORDER:
        if name in steps:
            steps[name]()
        elif name[0] == "S":
            fam = name[1]
            hop1_done(fam, t)
            if t < 4:
                hop1(fam, t + 1)
            else:
                ref = row_of(fam, second[fam], LA if fam == "A" else LB)
                send(ref, ref, partner, "P0", "P0")
            hop2("G" + fam, 1, t)
        elif name[0] == "P":
            to_partner(name[1:], t)
        else:
            if t > 0:
                hop2_done(name, t, q)
            if t < 4:
                hop2(name, t + 1, q)

    arrived(("f", 1), sb0.at[0:4])
    arrived(("d", 1), rb1)
    arrived(("d", 2), rb2)

    def put(i, lane, value):
        ffn[:, pl.ds(pl.multiple_of(place(i) * 256 + lane, 128), value.shape[-1])] = value

    for half in range(2):
        got = take0(0, half) + fl0[half].astype(F32) + fr0[half].astype(F32)
        for i in range(5):
            put(i, 128 * half, got[i])
    for lo, hi, rbuf in ((5, 7, rb1), (7, 8, rb2)):
        for i in range(lo, hi):
            put(i, 0, parts2[i, 0:BLK, :] + sum(rbuf[k, i - lo].astype(F32) for k in range(3)))
    out[...] = (stream[...] + 0.5 * rms_scale(ffn[...], og[...])).astype(BF16)

    for fam, lanes in (("A", LA), ("B", LB)):
        sent("S" + fam, W.at[c, 0, 0:7, :, lanes])
    for name in LANES:
        sent(name, W.at[c, 0:7, :, :, LANES[name]])
    sent("P0", W.at[c, 0, :, :, ALL])
    sent("PG", W.at[c, 0:7, :, :, GU])
    sent("PDB", W.at[c, 0:7, :, :, DB])
    for t, n in ((2, 4), (3, 2), (4, 1)):
        sent(("PDA", t), W.at[c, 0:n, :, :, DA])
    for out_, ref in (
        ("halo", halo), ("wp", wp.at[1]), ("row", rowbuf), ("col", colbuf), ("mix", mixb), (("sb", 0), sb),
        ("nb", sb), (("sb", 1), sb0), (("d", 1), sb1), (("d", 2), sb2),
    ):
        sent(out_, ref)
    assert len(recv_ids) <= NRECV and len(send_ids) <= NSEND, (len(recv_ids), len(send_ids))


def shards(
    resid, x_branch, gate_branch, conv_w, gate_a_w, gate_x_w, decay_rate, decay_extra, w_proj, mix_gain,
    pre_gain, w_gate, w_up, w_down, out_gain,
):
    vmem = pltpu.VMEM
    return pl.pallas_call(
        kernel,
        out_shape=jax.ShapeDtypeStruct((BLK, D), BF16),
        in_specs=[pl.BlockSpec(memory_space=pl.ANY)] * 15,
        out_specs=pl.BlockSpec(memory_space=pltpu.VMEM),
        scratch_shapes=[
            vmem((2, NF, NF, 32, WL), BF16),
            vmem((2, CH, D), BF16),
            vmem((ROWS, CH), BF16),
            vmem((ROWS + 16, CH), F32),
            vmem((ROWS, CH), BF16),
            vmem((ROWS, CH), F32),
            vmem((4, CH), F32),
            vmem((4, 64, 64), BF16),
            vmem((4, 64, 64), BF16),
            vmem((1, CH), F32),
            vmem((1, D), F32),
            vmem((1, D), F32),
            vmem((1, D), F32),
            vmem((32, HID), BF16),
            vmem((32, HID), BF16),
            vmem((32, HID), BF16),
            vmem((BLK, D), BF16),
            vmem((16, CH), BF16),
            vmem((CH, 2 * CH), BF16),
            vmem((ROWS, CH), BF16),
            vmem((ROWS, 2 * CH), F32),
            vmem((ROWS, CH), F32),
            vmem((ROWS, CH), F32),
            vmem((ROWS, CH), F32),
            vmem((1, 2 * CH), F32),
            vmem((NF - 1, 1, 2 * CH), F32),
            vmem((1, 2 * CH), F32),
            vmem((NF - 1, 1, 2 * CH), F32),
            vmem((NX * BLK, CH), BF16),
            vmem((NX * BLK, CH), BF16),
            vmem((NX * BLK, CH), BF16),
            vmem((NX * BLK, D), F32),
            vmem((BLK, D), F32),
            vmem((6, BLK, 1024), BF16),
            vmem((BLK, 1024), BF16),
            vmem((BLK, 1024), BF16),
            vmem((2, BLK, 1024), BF16),
            vmem((2, BLK, 1024), BF16),
            vmem((2, NX, BLK, 1024), BF16),
            vmem((2, NX * BLK, 768), BF16),
            vmem((NF, NX * BLK, 256), F32),
            vmem((6, 5, BLK, 128), BF16),
            vmem((5, BLK, 128), BF16),
            vmem((5, BLK, 128), BF16),
            vmem((2, 5, BLK, 128), BF16),
            vmem((2, 5, BLK, 128), BF16),
            vmem((3, 2, BLK, 256), BF16),
            vmem((3, 2, BLK, 256), BF16),
            vmem((3, 1, BLK, 256), BF16),
            vmem((3, 1, BLK, 256), BF16),
            vmem((BLK, D), F32),
            pltpu.SemaphoreType.DMA((15,)),
            pltpu.SemaphoreType.DMA((NSEND,)),
            pltpu.SemaphoreType.DMA((NRECV,)),
        ],
        compiler_params=pltpu.CompilerParams(
            collective_id=0, has_side_effects=True, vmem_limit_bytes=58 * 1024 * 1024
        ),
        name="layer",
    )(
        resid, x_branch, gate_branch, conv_w, gate_a_w, gate_x_w, decay_rate.reshape(1, CH), decay_extra,
        w_proj, mix_gain.reshape(1, D), pre_gain.reshape(1, D), w_gate, w_up, w_down.T, out_gain.reshape(1, D),
    )


def solution(mesh):
    return jax.shard_map(
        shards,
        mesh=mesh,
        in_specs=(
            P("sp", None),
            P("sp", "tp"),
            P("sp", "tp"),
            P(None, "tp"),
            P("tp", None, None),
            P("tp", None, None),
            P("tp"),
            P("sp", "tp"),
            P("tp", None),
            P(),
            P(),
            P("sp", "tp"),
            P("sp", "tp"),
            P("tp", "sp"),
            P(),
        ),
        out_specs=P(("sp", "tp"), None),
        check_vma=False,
    )
```

time: 101 us -> 90.7 us (0.90)
  Pallas kernels: 97.2 us -> 88.9 us
  local copies, waits for them, and re-layouts: 3.22 us -> 1.62 us
    pallas_call x1, Pallas kernels: 97.2 us -> 88.9 us  [shards(): pl.pallas_call(kernel, out_shape=jax.ShapeDtypeStruct((BLK, D), BF16), in...]
    unnamed x2 -> x1, local copies, waits for them, and re-layouts: 3.22 us -> 1.62 us
where the time goes in v2:
time: 90.7 us; the launch traced here: 90.5 us
  Pallas kernels  88.9 us (98%)
  local copies, waits for them, and re-layouts  1.62 us (2%)
    pallas_call x1, Pallas kernels, shards(): pl.pallas_call(kernel, out_shape=jax.ShapeDtypeStruct((BLK, D), BF16), in...  88.9 us

profile of v2, /device:TPU:1, one launch (start us, length us, event | category | flops | bytes accessed | tf_op | source)
XLA Modules:
  0.0 90.5 jit_solution(17180211641548182814)
XLA Ops:
  0.0 88.9 %layer.1 = bf16[48,2048]{1,0:T(8,128)(2,1)} custom-call(bf16[384,2048]{1,0:T(8,128)(2,1)} %resid.1, bf16[384,256]{1,0:T(8,128)(2,1)} %x_in.1, bf16[384,256]{1,0:T(8,128)(2,1)} %g_in.1, f32[4,256]{1,0:T(4,128)} %conv_w.1, bf16[4,64,64]{2,1,0:T(8,128)(2,1)} %ga_in.1, bf16[4,64,64]{2,1,0:T(8,128)(2,1)} %gx_in.1, f32[1,256]{1,0:T(1,128)} %bitcast.9, ...), custom_call_target="tpu_custom_call" | custom-call | tf_op jit(solution)/shard_map/layer/pallas_call | solution.py:528
  88.9 1.6 %copy.17 = bf16[48,2048]{1,0:T(8,128)(2,1)} copy(bf16[48,2048]{1,0:T(8,128)(2,1)} %layer.1) | data formatting | bytes 393216

commit v3 on v2

--- a/solution.py
+++ b/solution.py
@@ -21,34 +21,40 @@
 BLK = 48
 HID = 704
 WL = 2176
-DA, GA, GB, DB = slice(0, 512), slice(512, 1152), slice(1152, 1920), slice(1920, 2176)
-LA, LB, GU, ALL = slice(0, 1152), slice(1152, WL), slice(512, 1920), slice(0, WL)
-LANES = {"DA": DA, "GA": GA, "GB": GB, "DB": DB}
+LANES = {"DA": slice(0, 768), "GA": slice(768, 1152), "GB1": slice(1152, 1664), "GB2": slice(1664, 2176)}
+LA, LB, ALL = slice(0, 1152), slice(1152, WL), slice(0, WL)
 GROUPS = ((0,), (1, 2), (3, 4), (5, 6), (7,))
-NRECV = 110
-NSEND = 22
+NRECV = 114
+NSEND = 24
 
 ORDER = (
-    ("DA", 0, 0), ("DB", 0, 0), ("scan", 0, 0), ("SB", 1, 0), ("SA", 1, 0), ("GA", 1, 0), ("GB", 1, 0),
-    ("DA", 1, 0), ("DB", 1, 0), ("SB", 2, 0), ("GB", 1, 1), ("row", 0, 0), ("GA", 1, 1), ("SA", 2, 0),
-    ("GA", 2, 0), ("DA", 2, 0), ("GB", 2, 0), ("DB", 2, 0), ("SB", 3, 0), ("GB", 1, 2), ("GA", 2, 1),
-    ("col", 0, 0), ("mix", 0, 0), ("GB", 2, 1), ("GA", 1, 2), ("GA", 3, 0), ("SA", 3, 0), ("DA", 3, 0),
-    ("mix2", 0, 0), ("GB", 3, 0), ("SB", 4, 0), ("DB", 3, 0), ("GA", 3, 1), ("GB", 1, 3), ("GA", 2, 2),
-    ("relay", 0, 0), ("GA", 4, 0), ("GB", 2, 2), ("GA", 1, 3), ("DA", 4, 0), ("GB", 3, 1), ("GA", 4, 1),
-    ("SA", 4, 0), ("send", 0, 0), ("GB", 4, 0), ("GA", 3, 2), ("GB", 1, 4), ("PGB", 1, 0), ("DB", 4, 0),
-    ("DA", 0, 1), ("GA", 2, 3), ("GB", 2, 3), ("GA", 1, 4), ("PGA", 1, 0), ("GA", 4, 2), ("ag", 0, 0),
-    ("GB", 3, 2), ("DA", 1, 1), ("GB", 4, 1), ("DA", 0, 2), ("GA", 3, 3), ("GB", 2, 4), ("PGB", 2, 0),
-    ("GA", 2, 4), ("PGA", 2, 0), ("agend", 0, 0), ("DB", 0, 1), ("GB", 3, 3), ("DA", 2, 1), ("GB", 4, 2),
-    ("DB", 0, 2), ("DA", 1, 2), ("DB", 0, 3), ("GB", 3, 4), ("PGB", 3, 0), ("GA", 4, 3), ("DB", 1, 1),
-    ("GA", 3, 4), ("PGA", 3, 0), ("GB", 4, 3), ("DA", 0, 3), ("DB", 0, 4), ("DB", 1, 2), ("DA", 3, 1),
-    ("DB", 1, 3), ("GB", 4, 4), ("PGB", 4, 0), ("DA", 0, 4), ("DA", 2, 2), ("GA", 4, 4), ("PGA", 4, 0),
-    ("DB", 2, 1), ("DB", 1, 4), ("PDB", 1, 0), ("DB", 2, 2), ("DA", 1, 3), ("gw", 0, 0), ("gu0", 0, 0),
-    ("DB", 2, 3), ("gu1", 0, 0), ("DA", 4, 1), ("gu2", 0, 0), ("DB", 3, 1), ("DA", 1, 4), ("PDA", 1, 0),
-    ("DB", 2, 4), ("PDB", 2, 0), ("gu3", 0, 0), ("DB", 3, 2), ("gu4", 0, 0), ("DA", 3, 2), ("DB", 3, 3),
-    ("gu5", 0, 0), ("DA", 2, 3), ("DB", 4, 1), ("DB", 3, 4), ("PDB", 3, 0), ("DA", 2, 4), ("PDA", 2, 0),
-    ("DB", 4, 2), ("DB", 4, 3), ("DA", 4, 2), ("DB", 4, 4), ("PDB", 4, 0), ("DA", 3, 3), ("g0", 0, 0),
-    ("DA", 3, 4), ("PDA", 3, 0), ("DA", 4, 3), ("g1", 0, 0), ("DA", 4, 4), ("PDA", 4, 0), ("g2", 0, 0),
-    ("g0r", 0, 0),
+    ("GB2", 0, 0), ("DA", 0, 0), ("scan1", 0, 0), ("SB", 1, 0), ("GB2", 0, 1), ("SA", 1, 0), ("scan2", 0, 0),
+    ("GA", 1, 0), ("GB1", 1, 0), ("scan3", 0, 0), ("DA", 1, 0), ("GB2", 1, 0), ("SB", 2, 0), ("GB1", 1, 1),
+    ("GA", 1, 1), ("GB2", 1, 1), ("GA", 2, 0), ("DA", 2, 0), ("SA", 2, 0), ("GB1", 2, 0), ("SB", 3, 0),
+    ("GB2", 2, 0), ("GA", 2, 1), ("GA", 3, 0), ("QGA", 3, 0), ("GB1", 1, 2), ("DA", 3, 0), ("QDA", 3, 0),
+    ("row", 0, 0), ("GB1", 2, 1), ("GA", 1, 2), ("SB", 4, 0), ("GB2", 2, 1), ("DA", 0, 1), ("GA", 3, 1),
+    ("QGA", 3, 1), ("GA", 4, 0), ("QGA", 4, 0), ("DA", 4, 0), ("QDA", 4, 0), ("SA", 3, 0), ("GB1", 3, 0),
+    ("QGB1", 3, 0), ("GA", 2, 2), ("GB1", 1, 3), ("GB2", 3, 0), ("QGB2", 3, 0), ("col", 0, 0), ("mix", 0, 0),
+    ("DA", 0, 2), ("DA", 1, 1), ("GA", 4, 1), ("QGA", 4, 1), ("GB1", 2, 2), ("GA", 1, 3), ("mix2", 0, 0),
+    ("GB1", 3, 1), ("QGB1", 3, 1), ("GA", 3, 2), ("QGA", 3, 2), ("GB1", 1, 4), ("PGB1", 1, 0), ("GB2", 3, 1),
+    ("QGB2", 3, 1), ("DA", 1, 2), ("SA", 4, 0), ("GB1", 4, 0), ("QGB1", 4, 0), ("relay", 0, 0), ("DA", 2, 1),
+    ("GB1", 2, 3), ("GB2", 4, 0), ("QGB2", 4, 0), ("GA", 2, 3), ("GA", 4, 2), ("QGA", 4, 2), ("GB2", 0, 2),
+    ("GB1", 3, 2), ("QGB1", 3, 2), ("GB1", 4, 1), ("QGB1", 4, 1), ("GB1", 2, 4), ("PGB1", 2, 0), ("send", 0, 0),
+    ("DA", 2, 2), ("GB2", 4, 1), ("QGB2", 4, 1), ("GA", 1, 4), ("PGA", 1, 0), ("GB2", 0, 3), ("GB1", 3, 3),
+    ("QGB1", 3, 3), ("DA", 3, 1), ("QDA", 3, 1), ("GB2", 0, 4), ("GB2", 1, 2), ("GA", 3, 3), ("QGA", 3, 3),
+    ("GB1", 4, 2), ("QGB1", 4, 2), ("ag", 0, 0), ("GB1", 3, 4), ("QGB1", 3, 4), ("DA", 0, 3), ("DA", 3, 2),
+    ("QDA", 3, 2), ("GB2", 1, 3), ("GA", 2, 4), ("PGA", 2, 0), ("GB1", 4, 3), ("QGB1", 4, 3), ("DA", 4, 1),
+    ("QDA", 4, 1), ("GB2", 1, 4), ("PGB2", 1, 0), ("GA", 4, 3), ("QGA", 4, 3), ("agend", 0, 0), ("GB2", 2, 2),
+    ("DA", 0, 4), ("GB1", 4, 4), ("QGB1", 4, 4), ("DA", 1, 3), ("GB2", 2, 3), ("DA", 4, 2), ("QDA", 4, 2),
+    ("GB2", 2, 4), ("PGB2", 2, 0), ("GA", 3, 4), ("QGA", 3, 4), ("u1c0", 0, 0), ("DA", 1, 4), ("PDA", 1, 0),
+    ("GB2", 3, 2), ("QGB2", 3, 2), ("u1c1", 0, 0), ("GB2", 3, 3), ("QGB2", 3, 3), ("DA", 2, 3), ("GB2", 3, 4),
+    ("QGB2", 3, 4), ("GA", 4, 4), ("QGA", 4, 4), ("GB2", 4, 2), ("QGB2", 4, 2), ("DA", 2, 4), ("PDA", 2, 0),
+    ("GB2", 4, 3), ("QGB2", 4, 3), ("GB2", 4, 4), ("QGB2", 4, 4), ("u0c0", 0, 0), ("DA", 3, 3), ("QDA", 3, 3),
+    ("u0c1", 0, 0), ("e0", 0, 0), ("DA", 3, 4), ("QDA", 3, 4), ("e1", 0, 0), ("e2", 0, 0), ("u2c0", 0, 0),
+    ("e3", 0, 0), ("u2c1", 0, 0), ("DA", 4, 3), ("QDA", 4, 3), ("DA", 4, 4), ("QDA", 4, 4), ("e4", 0, 0),
+    ("f0", 0, 0), ("e5", 0, 0), ("f1", 0, 0), ("e6", 0, 0), ("f2", 0, 0), ("f3", 0, 0), ("g0s", 0, 0),
+    ("f4", 0, 0), ("f5", 0, 0), ("e7", 0, 0), ("f6", 0, 0), ("f7", 0, 0), ("g1s", 0, 0), ("g2s", 0, 0),
+    ("g0r", 0, 0), ("g1r", 0, 0),
 )
 
 
@@ -87,7 +93,7 @@
     W, wp, xb, xp, gb, eb, cw, ga, gx, rt, mg, pg, og, wg, wu, wd, rs_b,
     halo, bd, cout, gates, acum, bcum, geb, tot, rowbuf, rtot, colbuf,
     mixa, mixs, mixb, parts, stream, sb, rl, rr, fl, fr, nb, hid,
-    parts2, sb0, rl0, rr0, fl0, fr0, sb1, rb1, sb2, rb2, ffn,
+    parts2, sb0, rl0, rr0, fl0, fr0, sb1, rl1, rr1, fl1, fr1, sb2, rb2, ffn,
     local_sem, send_sem, recv_sem,
 ):
     sp = lax.axis_index("sp")
@@ -138,15 +144,14 @@
     for name in ("wg", "wu", "wd"):
         loads[name].wait()
     mine = W.at[c, z, y]
-    mine[:, 0:512] = wd[:, 0:512]
+    mine[:, 0:640] = wd[:, 0:640]
+    mine[:, 640:768] = jnp.concatenate([wd[:, 640:704], jnp.zeros((32, 64), BF16)], axis=1)
+    mine[:, 768:896] = wg[:, 512:640]
+    mine[:, 896:1024] = wu[:, 512:640]
+    mine[:, 1024:1152] = jnp.concatenate([wg[:, 640:704], wu[:, 640:704]], axis=1)
     for n in range(2):
-        mine[:, 512 * n + 512 : 512 * n + 768] = wg[:, 256 * n : 256 * n + 256]
-        mine[:, 512 * n + 768 : 512 * n + 1024] = wu[:, 256 * n : 256 * n + 256]
-    mine[:, 1536:1664] = wg[:, 512:640]
-    mine[:, 1664:1792] = wu[:, 512:640]
-    mine[:, 1792:1920] = jnp.concatenate([wg[:, 640:704], wu[:, 640:704]], axis=1)
-    mine[:, 1920:2048] = wd[:, 512:640]
-    mine[:, 2048:2176] = jnp.concatenate([wd[:, 640:704], jnp.zeros((32, 64), BF16)], axis=1)
+        mine[:, 512 * n + 1152 : 512 * n + 1408] = wg[:, 256 * n : 256 * n + 256]
+        mine[:, 512 * n + 1408 : 512 * n + 1664] = wu[:, 256 * n : 256 * n + 256]
 
     send_ids, recv_ids = {}, {}
 
@@ -220,20 +225,30 @@
         n = len(GROUPS[q])
         arrived((name, t, q), some(2 * n if t < 4 else n, LANES[name]))
 
+    def partner_ids(name, t):
+        to = ("PDA", t) if name == "DA" else "P" + name
+        return to, to
+
     def to_partner(name, t):
         fam = name[1]
         for sign in (-1, 1)[: 2 if t < 4 else 1]:
             ref = row_of(fam, mod(second[fam] + sign * t), LANES[name])
-            to = "PG" if name[0] == "G" else ("PDB" if fam == "B" else ("PDA", max(t, 2)))
-            send(ref, ref, partner, to, to)
+            send(ref, ref, partner, *partner_ids(name, t))
+
+    def group_to_partner(name, t, q):
+        fam = name[1]
+        for sign in (-1, 1)[: 2 if t < 4 else 1]:
+            for j in GROUPS[q]:
+                ref = piece(fam, mod(first[fam] + offset(j)), mod(second[fam] + sign * t), LANES[name])
+                send(ref, ref, partner, *partner_ids(name, t))
 
     loads["x"].wait()
     pl.semaphore_wait(barrier, len(peers))
+    send(xb.at[pl.ds(ROWS - 16, 16), :], halo, ahead, "halo", "halo")
     hop1("A", 1)
     hop1("B", 1)
-    send(xb.at[pl.ds(ROWS - 16, 16), :], halo, ahead, "halo", "halo")
     hop2("GA", 1, 0)
-    hop2("GB", 1, 0)
+    hop2("GB1", 1, 0)
     loads["wp"].wait()
     send(wp.at[0], wp.at[1], partner, "wp", "wp")
     for name in ("ga", "gx", "g", "cw", "rt", "e"):
@@ -246,7 +261,7 @@
     xp[16:, :] = xb[...].astype(F32)
     geb[...] = gelu(gb[...].astype(F32))
 
-    def scan():
+    def scan1():
         arrived("halo", halo)
         xp[0:16, :] = jnp.where(sp > 0, halo[...].astype(F32), 0.0)
         conv = xp[13 : 13 + ROWS, :] * cw[0:1, :]
@@ -254,6 +269,10 @@
             conv = conv + xp[13 + tap : 13 + tap + ROWS, :] * cw[tap : tap + 1, :]
         cout[...] = conv.astype(BF16)
         gates[...] = dot(cout[...], bd[...])
+
+    held = {}
+
+    def scan_rows(lo, hi, start):
         in_group = lax.broadcasted_iota(jnp.int32, (4, 8, CH), 1)
 
         def chunk(i, carry):
@@ -285,8 +304,13 @@
             bcum[rows, :] = jnp.concatenate(b_all, axis=0)
             return a_in, b_in
 
-        start = (jnp.ones((1, CH), F32), jnp.zeros((1, CH), F32))
-        a_end, b_end = lax.fori_loop(0, ROWS // 32, chunk, start)
+        return lax.fori_loop(lo, hi, chunk, start)
+
+    def scan2():
+        held["half"] = scan_rows(0, 6, (jnp.ones((1, CH), F32), jnp.zeros((1, CH), F32)))
+
+    def scan3():
+        a_end, b_end = scan_rows(6, ROWS // 32, held["half"])
         tot[:, 0:CH] = a_end
         tot[:, CH:] = b_end
         for k in range(1, NF):
@@ -305,8 +329,6 @@
             eb_ = jnp.where(is_me, pb, eb_)
             pa, pb = pa * va, va * pb + vb
         return (pa, pb), (ea, eb_)
-
-    held = {}
 
     def row():
         arrived("row", rowbuf)
@@ -394,24 +416,28 @@
     def agend():
         arrived("ab", nb.at[0])
 
-    def gw():
-        arrived("P0", W.at[c, 0, :, :, ALL])
-        arrived("PG", W.at[c, 0:7, :, :, GU])
-
     def gate_up(core, lanes):
         w = W[core, :, :, :, lanes]
         w = w.reshape(D, w.shape[-1])
         acc = dot(nb[0].reshape(NX * BLK, 1024), w[0:1024])
         return acc + dot(nb[1].reshape(NX * BLK, 1024), w[1024:])
 
-    def gu(i):
-        core, n = i // 3, i % 3
-        if n < 2:
-            both = gate_up(core, slice(512 * n + 512, 512 * n + 1024))
+    came = set()
+
+    def came_from_partner(to, like):
+        if to not in came:
+            came.add(to)
+            arrived(to, like)
+
+    def gate_and_up(n, core):
+        name = ("GA", "GB1", "GB2")[n]
+        came_from_partner("P0", W.at[c, 0, :, :, ALL])
+        came_from_partner("P" + name, W.at[c, 0:7, :, :, LANES[name]])
+        both = gate_up(core, LANES[name])
+        if n > 0:
             g, u = both[:, 0:256], both[:, 256:512]
-            hid[core, :, 256 * n : 256 * n + 256] = (g * sigmoid(g) * u).astype(BF16)
+            hid[core, :, 256 * n - 256 : 256 * n] = (g * sigmoid(g) * u).astype(BF16)
         else:
-            both = gate_up(core, slice(1536, 1920))
             g, u = both[:, 0:128], both[:, 128:256]
             hid[core, :, 512:640] = (g * sigmoid(g) * u).astype(BF16)
             g = both[:, 256:384]
@@ -422,50 +448,59 @@
     def place(i):
         return (z + NF + (i + 1) // 2 * (1 - 2 * (i % 2))) % NF
 
-    def down(i, _):
+    def down(i, parts_of_k):
         acc = jnp.zeros((NX * BLK, 256), F32)
         for core in range(2):
-            wa = W[core, place(i), :, :, DA].reshape(256, 512)
-            wb = W[core, place(i), :, :, DB].reshape(256, 256)
-            acc = acc + dot_nt(hid[core, :, 0:512], wa) + dot_nt(hid[core, :, 512:768], wb)
-        parts2[i] = acc
-        return 0
+            for lanes in parts_of_k:
+                w = W[core, place(i), :, :, lanes]
+                acc = acc + dot_nt(hid[core, :, lanes], w.reshape(256, lanes.stop - lanes.start))
+        return acc
+
+    def down_first(i):
+        if i > 0:
+            came_from_partner(("PDA", (i + 1) // 2), W.at[c, 0 : 2 if i < 7 else 1, :, :, LANES["DA"]])
+        parts2[i] = down(i, (slice(0, 256), slice(512, 768)))
+
+    def down_last(i):
+        parts2[i] += down(i, (slice(256, 512),))
 
     bufs0 = (rl0, rr0, fl0, fr0)
+    bufs1 = (rl1, rr1, fl1, fr1)
 
     def take0(rel, half):
-        return parts2[0:5, BLK * rel : BLK * rel + BLK, 128 * half : 128 * half + 128]
-
-    def g0():
-        arrived("PDB", W.at[c, 0:7, :, :, DB])
-        arrived(("PDA", 2), W.at[c, 0:4, :, :, DA])
-        lax.fori_loop(0, 5, down, 0)
+        return parts2[0:3, BLK * rel : BLK * rel + BLK, 128 * half : 128 * half + 128]
+
+    def take1(rel, half):
+        return parts2[3:7, BLK * rel : BLK * rel + BLK, 128 * half : 128 * half + 128]
+
+    def g0s():
         scatter_start(1, take0, sb0, bufs0)
 
     def g0r():
         scatter_relay(1, take0, sb0, bufs0)
 
-    def direct(u, lo, hi, sbuf, rbuf):
+    def g1s():
+        scatter_start(2, take1, sb1, bufs1)
+
+    def g1r():
+        scatter_relay(2, take1, sb1, bufs1)
+
+    def g2s():
         for k, (rel, step) in enumerate(((2, 2), (1, 1), (3, NX - 1))):
-            sbuf[k] = parts2[lo:hi, BLK * rel : BLK * rel + BLK, :].astype(BF16)
-            send(sbuf.at[k], rbuf.at[k], at_x(step), ("d", u), ("d", u))
-
-    def g1():
-        arrived(("PDA", 3), W.at[c, 0:2, :, :, DA])
-        lax.fori_loop(5, 7, down, 0)
-        direct(1, 5, 7, sb1, rb1)
-
-    def g2():
-        arrived(("PDA", 4), W.at[c, 0, :, :, DA])
-        down(7, 0)
-        direct(2, 7, 8, sb2, rb2)
+            sb2[k] = parts2[7, BLK * rel : BLK * rel + BLK, :].astype(BF16)
+            send(sb2.at[k], rb2.at[k], at_x(step), "d", "d")
 
     steps = {
-        "scan": scan, "row": row, "col": col, "mix": mix, "mix2": mix2, "relay": relay, "send": norm_and_send,
-        "ag": ag, "agend": agend, "gw": gw, "g0": g0, "g0r": g0r, "g1": g1, "g2": g2,
+        "scan1": scan1, "scan2": scan2, "scan3": scan3, "row": row, "col": col, "mix": mix, "mix2": mix2,
+        "relay": relay, "send": norm_and_send, "ag": ag, "agend": agend, "g0s": g0s, "g0r": g0r, "g1s": g1s,
+        "g1r": g1r, "g2s": g2s,
     }
-    for i in range(6):
-        steps["gu%d" % i] = functools.partial(gu, i)
+    for n in range(3):
+        for core in range(2):
+            steps["u%dc%d" % (n, core)] = functools.partial(gate_and_up, n, core)
+    for i in range(NF):
+        steps["e%d" % i] = functools.partial(down_first, i)
+        steps["f%d" % i] = functools.partial(down_last, i)
 
     for name, t, q in ORDER:
         if name in steps:
@@ -478,29 +513,28 @@
             else:
                 ref = row_of(fam, second[fam], LA if fam == "A" else LB)
                 send(ref, ref, partner, "P0", "P0")
-            hop2("G" + fam, 1, t)
+            hop2("GA" if fam == "A" else "GB1", 1, t)
         elif name[0] == "P":
             to_partner(name[1:], t)
+        elif name[0] == "Q":
+            group_to_partner(name[1:], t, q)
         else:
             if t > 0:
                 hop2_done(name, t, q)
             if t < 4:
                 hop2(name, t + 1, q)
 
-    arrived(("f", 1), sb0.at[0:4])
-    arrived(("d", 1), rb1)
-    arrived(("d", 2), rb2)
-
     def put(i, lane, value):
         ffn[:, pl.ds(pl.multiple_of(place(i) * 256 + lane, 128), value.shape[-1])] = value
 
-    for half in range(2):
-        got = take0(0, half) + fl0[half].astype(F32) + fr0[half].astype(F32)
-        for i in range(5):
-            put(i, 128 * half, got[i])
-    for lo, hi, rbuf in ((5, 7, rb1), (7, 8, rb2)):
-        for i in range(lo, hi):
-            put(i, 0, parts2[i, 0:BLK, :] + sum(rbuf[k, i - lo].astype(F32) for k in range(3)))
+    for u, lo, hi, take_, sbuf, (_, _, fl_, fr_) in ((1, 0, 3, take0, sb0, bufs0), (2, 3, 7, take1, sb1, bufs1)):
+        arrived(("f", u), sbuf.at[0:4])
+        for half in range(2):
+            got = take_(0, half) + fl_[half].astype(F32) + fr_[half].astype(F32)
+            for i in range(lo, hi):
+                put(i, 128 * half, got[i - lo])
+    arrived("d", rb2)
+    put(7, 0, parts2[7, 0:BLK, :] + sum(rb2[k].astype(F32) for k in range(3)))
     out[...] = (stream[...] + 0.5 * rms_scale(ffn[...], og[...])).astype(BF16)
 
     for fam, lanes in (("A", LA), ("B", LB)):
@@ -508,13 +542,13 @@
     for name in LANES:
         sent(name, W.at[c, 0:7, :, :, LANES[name]])
     sent("P0", W.at[c, 0, :, :, ALL])
-    sent("PG", W.at[c, 0:7, :, :, GU])
-    sent("PDB", W.at[c, 0:7, :, :, DB])
-    for t, n in ((2, 4), (3, 2), (4, 1)):
-        sent(("PDA", t), W.at[c, 0:n, :, :, DA])
+    for name in ("GA", "GB1", "GB2"):
+        sent("P" + name, W.at[c, 0:7, :, :, LANES[name]])
+    for t, n in ((1, 2), (2, 2), (3, 2), (4, 1)):
+        sent(("PDA", t), W.at[c, 0:n, :, :, LANES["DA"]])
     for out_, ref in (
         ("halo", halo), ("wp", wp.at[1]), ("row", rowbuf), ("col", colbuf), ("mix", mixb), (("sb", 0), sb),
-        ("nb", sb), (("sb", 1), sb0), (("d", 1), sb1), (("d", 2), sb2),
+        ("nb", sb), (("sb", 1), sb0), (("sb", 2), sb1), ("d", sb2),
     ):
         sent(out_, ref)
     assert len(recv_ids) <= NRECV and len(send_ids) <= NSEND, (len(recv_ids), len(send_ids))
@@ -572,15 +606,18 @@
             vmem((2, NX, BLK, 1024), BF16),
             vmem((2, NX * BLK, 768), BF16),
             vmem((NF, NX * BLK, 256), F32),
-            vmem((6, 5, BLK, 128), BF16),
-            vmem((5, BLK, 128), BF16),
-            vmem((5, BLK, 128), BF16),
-            vmem((2, 5, BLK, 128), BF16),
-            vmem((2, 5, BLK, 128), BF16),
-            vmem((3, 2, BLK, 256), BF16),
-            vmem((3, 2, BLK, 256), BF16),
-            vmem((3, 1, BLK, 256), BF16),
-            vmem((3, 1, BLK, 256), BF16),
+            vmem((6, 3, BLK, 128), BF16),
+            vmem((3, BLK, 128), BF16),
+            vmem((3, BLK, 128), BF16),
+            vmem((2, 3, BLK, 128), BF16),
+            vmem((2, 3, BLK, 128), BF16),
+            vmem((6, 4, BLK, 128), BF16),
+            vmem((4, BLK, 128), BF16),
+            vmem((4, BLK, 128), BF16),
+            vmem((2, 4, BLK, 128), BF16),
+            vmem((2, 4, BLK, 128), BF16),
+            vmem((3, BLK, 256), BF16),
+            vmem((3, BLK, 256), BF16),
             vmem((BLK, D), F32),
             pltpu.SemaphoreType.DMA((15,)),
             pltpu.SemaphoreType.DMA((NSEND,)),

time: 90.7 us -> 87.5 us (0.965)
  Pallas kernels: 88.9 us -> 85.7 us
    pallas_call x1, Pallas kernels: 88.9 us -> 85.7 us  [shards(): pl.pallas_call(kernel, out_shape=jax.ShapeDtypeStruct((BLK, D), BF16), in...]
where the time goes in v3:
time: 87.5 us; the launch traced here: 87.3 us
  Pallas kernels  85.7 us (98%)
  local copies, waits for them, and re-layouts  1.62 us (2%)
    pallas_call x1, Pallas kernels, shards(): pl.pallas_call(kernel, out_shape=jax.ShapeDtypeStruct((BLK, D), BF16), in...  85.7 us

profile of v3, /device:TPU:1, one launch (start us, length us, event | category | flops | bytes accessed | tf_op | source)
XLA Modules:
  0.0 87.3 jit_solution(16186788052278547375)
XLA Ops:
  0.0 85.7 %layer.1 = bf16[48,2048]{1,0:T(8,128)(2,1)} custom-call(bf16[384,2048]{1,0:T(8,128)(2,1)} %resid.1, bf16[384,256]{1,0:T(8,128)(2,1)} %x_in.1, bf16[384,256]{1,0:T(8,128)(2,1)} %g_in.1, f32[4,256]{1,0:T(4,128)} %conv_w.1, bf16[4,64,64]{2,1,0:T(8,128)(2,1)} %ga_in.1, bf16[4,64,64]{2,1,0:T(8,128)(2,1)} %gx_in.1, f32[1,256]{1,0:T(1,128)} %bitcast.9, ...), custom_call_target="tpu_custom_call" | custom-call | tf_op jit(solution)/shard_map/layer/pallas_call | solution.py:562
  85.7 1.6 %copy.17 = bf16[48,2048]{1,0:T(8,128)(2,1)} copy(bf16[48,2048]{1,0:T(8,128)(2,1)} %layer.1) | data formatting | bytes 393216

commit v4 on v3

--- a/solution.py
+++ b/solution.py
@@ -22,38 +22,32 @@
 HID = 704
 WL = 2176
 LANES = {"DA": slice(0, 768), "GA": slice(768, 1152), "GB1": slice(1152, 1664), "GB2": slice(1664, 2176)}
-LA, LB, ALL = slice(0, 1152), slice(1152, WL), slice(0, WL)
+LA, LB = slice(0, 1152), slice(1152, WL)
 GROUPS = ((0,), (1, 2), (3, 4), (5, 6), (7,))
-NRECV = 114
-NSEND = 24
+NRECV = 111
+NSEND = 21
 
 ORDER = (
-    ("GB2", 0, 0), ("DA", 0, 0), ("scan1", 0, 0), ("SB", 1, 0), ("GB2", 0, 1), ("SA", 1, 0), ("scan2", 0, 0),
-    ("GA", 1, 0), ("GB1", 1, 0), ("scan3", 0, 0), ("DA", 1, 0), ("GB2", 1, 0), ("SB", 2, 0), ("GB1", 1, 1),
-    ("GA", 1, 1), ("GB2", 1, 1), ("GA", 2, 0), ("DA", 2, 0), ("SA", 2, 0), ("GB1", 2, 0), ("SB", 3, 0),
-    ("GB2", 2, 0), ("GA", 2, 1), ("GA", 3, 0), ("QGA", 3, 0), ("GB1", 1, 2), ("DA", 3, 0), ("QDA", 3, 0),
-    ("row", 0, 0), ("GB1", 2, 1), ("GA", 1, 2), ("SB", 4, 0), ("GB2", 2, 1), ("DA", 0, 1), ("GA", 3, 1),
-    ("QGA", 3, 1), ("GA", 4, 0), ("QGA", 4, 0), ("DA", 4, 0), ("QDA", 4, 0), ("SA", 3, 0), ("GB1", 3, 0),
-    ("QGB1", 3, 0), ("GA", 2, 2), ("GB1", 1, 3), ("GB2", 3, 0), ("QGB2", 3, 0), ("col", 0, 0), ("mix", 0, 0),
-    ("DA", 0, 2), ("DA", 1, 1), ("GA", 4, 1), ("QGA", 4, 1), ("GB1", 2, 2), ("GA", 1, 3), ("mix2", 0, 0),
-    ("GB1", 3, 1), ("QGB1", 3, 1), ("GA", 3, 2), ("QGA", 3, 2), ("GB1", 1, 4), ("PGB1", 1, 0), ("GB2", 3, 1),
-    ("QGB2", 3, 1), ("DA", 1, 2), ("SA", 4, 0), ("GB1", 4, 0), ("QGB1", 4, 0), ("relay", 0, 0), ("DA", 2, 1),
-    ("GB1", 2, 3), ("GB2", 4, 0), ("QGB2", 4, 0), ("GA", 2, 3), ("GA", 4, 2), ("QGA", 4, 2), ("GB2", 0, 2),
-    ("GB1", 3, 2), ("QGB1", 3, 2), ("GB1", 4, 1), ("QGB1", 4, 1), ("GB1", 2, 4), ("PGB1", 2, 0), ("send", 0, 0),
-    ("DA", 2, 2), ("GB2", 4, 1), ("QGB2", 4, 1), ("GA", 1, 4), ("PGA", 1, 0), ("GB2", 0, 3), ("GB1", 3, 3),
-    ("QGB1", 3, 3), ("DA", 3, 1), ("QDA", 3, 1), ("GB2", 0, 4), ("GB2", 1, 2), ("GA", 3, 3), ("QGA", 3, 3),
-    ("GB1", 4, 2), ("QGB1", 4, 2), ("ag", 0, 0), ("GB1", 3, 4), ("QGB1", 3, 4), ("DA", 0, 3), ("DA", 3, 2),
-    ("QDA", 3, 2), ("GB2", 1, 3), ("GA", 2, 4), ("PGA", 2, 0), ("GB1", 4, 3), ("QGB1", 4, 3), ("DA", 4, 1),
-    ("QDA", 4, 1), ("GB2", 1, 4), ("PGB2", 1, 0), ("GA", 4, 3), ("QGA", 4, 3), ("agend", 0, 0), ("GB2", 2, 2),
-    ("DA", 0, 4), ("GB1", 4, 4), ("QGB1", 4, 4), ("DA", 1, 3), ("GB2", 2, 3), ("DA", 4, 2), ("QDA", 4, 2),
-    ("GB2", 2, 4), ("PGB2", 2, 0), ("GA", 3, 4), ("QGA", 3, 4), ("u1c0", 0, 0), ("DA", 1, 4), ("PDA", 1, 0),
-    ("GB2", 3, 2), ("QGB2", 3, 2), ("u1c1", 0, 0), ("GB2", 3, 3), ("QGB2", 3, 3), ("DA", 2, 3), ("GB2", 3, 4),
-    ("QGB2", 3, 4), ("GA", 4, 4), ("QGA", 4, 4), ("GB2", 4, 2), ("QGB2", 4, 2), ("DA", 2, 4), ("PDA", 2, 0),
-    ("GB2", 4, 3), ("QGB2", 4, 3), ("GB2", 4, 4), ("QGB2", 4, 4), ("u0c0", 0, 0), ("DA", 3, 3), ("QDA", 3, 3),
-    ("u0c1", 0, 0), ("e0", 0, 0), ("DA", 3, 4), ("QDA", 3, 4), ("e1", 0, 0), ("e2", 0, 0), ("u2c0", 0, 0),
-    ("e3", 0, 0), ("u2c1", 0, 0), ("DA", 4, 3), ("QDA", 4, 3), ("DA", 4, 4), ("QDA", 4, 4), ("e4", 0, 0),
-    ("f0", 0, 0), ("e5", 0, 0), ("f1", 0, 0), ("e6", 0, 0), ("f2", 0, 0), ("f3", 0, 0), ("g0s", 0, 0),
-    ("f4", 0, 0), ("f5", 0, 0), ("e7", 0, 0), ("f6", 0, 0), ("f7", 0, 0), ("g1s", 0, 0), ("g2s", 0, 0),
+    ("GB1", 0, 0), ("GA", 0, 0), ("GB2", 0, 0), ("DA", 0, 0), ("scan1", 0, 0), ("SB", 1, 0), ("GB1", 0, 1),
+    ("SA", 1, 0), ("scan2", 0, 0), ("GA", 0, 1), ("scan3", 0, 0), ("GB1", 1, 0), ("GA", 1, 0), ("DA", 0, 1),
+    ("GB2", 0, 1), ("SB", 2, 0), ("GB1", 0, 2), ("GB1", 1, 1), ("SA", 2, 0), ("GA", 1, 1), ("GA", 2, 0),
+    ("GA", 0, 2), ("GB1", 2, 0), ("row", 0, 0), ("DA", 1, 0), ("SB", 3, 0), ("GB1", 0, 3), ("GA", 2, 1),
+    ("GB1", 1, 2), ("GA", 3, 0), ("GB1", 2, 1), ("GA", 1, 2), ("SA", 3, 0), ("GA", 0, 3), ("DA", 0, 2),
+    ("SB", 4, 0), ("GB1", 3, 0), ("GB1", 0, 4), ("col", 0, 0), ("GB1", 1, 3), ("GA", 3, 1), ("GA", 4, 0),
+    ("mix", 0, 0), ("GA", 2, 2), ("GB1", 2, 2), ("GA", 1, 3), ("mix2", 0, 0), ("GB1", 3, 1), ("SA", 4, 0),
+    ("GA", 0, 4), ("GB1", 4, 0), ("DA", 1, 1), ("GB1", 1, 4), ("GA", 4, 1), ("GB2", 1, 0), ("GB1", 2, 3),
+    ("GA", 3, 2), ("DA", 0, 3), ("GB1", 3, 2), ("relay", 0, 0), ("GB1", 4, 1), ("GB2", 0, 2), ("GA", 2, 3),
+    ("GB1", 2, 4), ("GA", 1, 4), ("GB2", 1, 1), ("GA", 4, 2), ("DA", 2, 0), ("GB1", 3, 3), ("GB1", 4, 2),
+    ("DA", 0, 4), ("send", 0, 0), ("GB2", 0, 3), ("DA", 1, 2), ("GB1", 3, 4), ("GA", 3, 3), ("GB2", 0, 4),
+    ("GA", 2, 4), ("GB2", 2, 0), ("GB2", 1, 2), ("GB1", 4, 3), ("DA", 2, 1), ("ag", 0, 0), ("GB2", 2, 1),
+    ("GB1", 4, 4), ("DA", 1, 3), ("GB2", 1, 3), ("GA", 4, 3), ("ag2", 0, 0), ("GA", 3, 4), ("GB2", 1, 4),
+    ("GB2", 3, 0), ("DA", 3, 0), ("GB2", 2, 2), ("DA", 1, 4), ("agend", 0, 0), ("DA", 2, 2), ("GB2", 3, 1),
+    ("GB2", 2, 3), ("agp", 0, 0), ("u1", 0, 0), ("DA", 3, 1), ("GB2", 2, 4), ("GA", 4, 4), ("GB2", 4, 0),
+    ("DA", 4, 0), ("u0", 0, 0), ("DA", 2, 3), ("GB2", 3, 2), ("GB2", 4, 1), ("DA", 2, 4), ("e0", 0, 0),
+    ("DA", 3, 2), ("GB2", 3, 3), ("GB2", 3, 4), ("DA", 4, 1), ("GB2", 4, 2), ("DA", 3, 3), ("GB2", 4, 3),
+    ("GB2", 4, 4), ("u2p", 0, 0), ("DA", 3, 4), ("f0p", 0, 0), ("e1", 0, 0), ("DA", 4, 2), ("h0", 0, 0),
+    ("f1p", 0, 0), ("h1", 0, 0), ("u2o", 0, 0), ("DA", 4, 3), ("f0o", 0, 0), ("DA", 4, 4), ("f1o", 0, 0),
+    ("g0s", 0, 0), ("e2", 0, 0), ("g1s", 0, 0), ("f2p", 0, 0), ("h2", 0, 0), ("f2o", 0, 0), ("g2s", 0, 0),
     ("g0r", 0, 0), ("g1r", 0, 0),
 )
 
@@ -93,7 +87,7 @@
     W, wp, xb, xp, gb, eb, cw, ga, gx, rt, mg, pg, og, wg, wu, wd, rs_b,
     halo, bd, cout, gates, acum, bcum, geb, tot, rowbuf, rtot, colbuf,
     mixa, mixs, mixb, parts, stream, sb, rl, rr, fl, fr, nb, hid,
-    parts2, sb0, rl0, rr0, fl0, fr0, sb1, rl1, rr1, fl1, fr1, sb2, rb2, ffn,
+    parts2, psend, pbuf, sb0, rl0, rr0, fl0, fr0, sb1, rl1, rr1, fl1, fr1, sb2, rb2, ffn,
     local_sem, send_sem, recv_sem,
 ):
     sp = lax.axis_index("sp")
@@ -143,7 +137,7 @@
 
     for name in ("wg", "wu", "wd"):
         loads[name].wait()
-    mine = W.at[c, z, y]
+    mine = W.at[z, y]
     mine[:, 0:640] = wd[:, 0:640]
     mine[:, 640:768] = jnp.concatenate([wd[:, 640:704], jnp.zeros((32, 64), BF16)], axis=1)
     mine[:, 768:896] = wg[:, 512:640]
@@ -176,13 +170,10 @@
         return (v + NF) % NF
 
     def piece(fam, first, second, lanes):
-        return W.at[c, second, first, :, lanes] if fam == "A" else W.at[c, first, second, :, lanes]
-
-    def row_of(fam, second, lanes):
-        return W.at[c, second, :, :, lanes] if fam == "A" else W.at[c, :, second, :, lanes]
+        return W.at[second, first, :, lanes] if fam == "A" else W.at[first, second, :, lanes]
 
     def some(n, lanes):
-        return W.at[c, 0, 0:n, :, lanes]
+        return W.at[0, 0:n, :, lanes]
 
     first = {"A": y, "B": z}
     second = {"A": z, "B": y}
@@ -225,30 +216,11 @@
         n = len(GROUPS[q])
         arrived((name, t, q), some(2 * n if t < 4 else n, LANES[name]))
 
-    def partner_ids(name, t):
-        to = ("PDA", t) if name == "DA" else "P" + name
-        return to, to
-
-    def to_partner(name, t):
-        fam = name[1]
-        for sign in (-1, 1)[: 2 if t < 4 else 1]:
-            ref = row_of(fam, mod(second[fam] + sign * t), LANES[name])
-            send(ref, ref, partner, *partner_ids(name, t))
-
-    def group_to_partner(name, t, q):
-        fam = name[1]
-        for sign in (-1, 1)[: 2 if t < 4 else 1]:
-            for j in GROUPS[q]:
-                ref = piece(fam, mod(first[fam] + offset(j)), mod(second[fam] + sign * t), LANES[name])
-                send(ref, ref, partner, *partner_ids(name, t))
-
     loads["x"].wait()
     pl.semaphore_wait(barrier, len(peers))
     send(xb.at[pl.ds(ROWS - 16, 16), :], halo, ahead, "halo", "halo")
     hop1("A", 1)
     hop1("B", 1)
-    hop2("GA", 1, 0)
-    hop2("GB1", 1, 0)
     loads["wp"].wait()
     send(wp.at[0], wp.at[1], partner, "wp", "wp")
     for name in ("ga", "gx", "g", "cw", "rt", "e"):
@@ -404,88 +376,107 @@
         nb[1, 0] = normed[:, 1024:]
         send(nb.at[0, 0], nb.at[0, 3], at_x(1), "al", "nb")
         send(nb.at[1, 0], nb.at[1, 1], at_x(NX - 1), "ar", "nb")
-        send(nb.at[1, 0], nb.at[1, 3], at_x(1), "ab", "nb")
-        send(nb.at[0, 0], nb.at[0, 1], at_x(NX - 1), "ab", "nb")
+        send(nb.at[1, 0], nb.at[1, 3], at_x(1), "an", "nb")
+        send(nb.at[0, 0], nb.at[0, 1], at_x(NX - 1), "an", "nb")
+        for half in range(2):
+            to_partner(half, 0)
+
+    def to_partner(half, rel):
+        send(nb.at[half, rel], nb.at[half, NX + rel], partner, "nbp", "nbp")
 
     def ag():
         arrived("al", nb.at[0, 3])
         send(nb.at[0, 3], nb.at[0, 2], at_x(1), "ab", "nb")
+        to_partner(0, 3)
         arrived("ar", nb.at[1, 1])
         send(nb.at[1, 1], nb.at[1, 2], at_x(NX - 1), "ab", "nb")
+        to_partner(1, 1)
+
+    def ag2():
+        arrived("an", nb.at[0, 0:2])
+        to_partner(1, 3)
+        to_partner(0, 1)
 
     def agend():
-        arrived("ab", nb.at[0])
-
-    def gate_up(core, lanes):
-        w = W[core, :, :, :, lanes]
+        arrived("ab", nb.at[0, 0:2])
+        to_partner(0, 2)
+        to_partner(1, 2)
+
+    def agp():
+        arrived("nbp", nb.at[0])
+
+    HALF = NX * BLK
+    mine_rows, other_rows, all_rows = slice(0, HALF), slice(HALF, 2 * HALF), slice(0, 2 * HALF)
+
+    def gate_up(n, span):
+        w = W[:, :, :, LANES[("GA", "GB1", "GB2")[n]]]
         w = w.reshape(D, w.shape[-1])
-        acc = dot(nb[0].reshape(NX * BLK, 1024), w[0:1024])
-        return acc + dot(nb[1].reshape(NX * BLK, 1024), w[1024:])
-
-    came = set()
-
-    def came_from_partner(to, like):
-        if to not in came:
-            came.add(to)
-            arrived(to, like)
-
-    def gate_and_up(n, core):
-        name = ("GA", "GB1", "GB2")[n]
-        came_from_partner("P0", W.at[c, 0, :, :, ALL])
-        came_from_partner("P" + name, W.at[c, 0:7, :, :, LANES[name]])
-        both = gate_up(core, LANES[name])
+        rows = span.stop - span.start
+        at = slice(span.start // BLK, span.stop // BLK)
+        both = dot(nb[0, at].reshape(rows, 1024), w[0:1024]) + dot(nb[1, at].reshape(rows, 1024), w[1024:])
         if n > 0:
             g, u = both[:, 0:256], both[:, 256:512]
-            hid[core, :, 256 * n - 256 : 256 * n] = (g * sigmoid(g) * u).astype(BF16)
+            hid[span, 256 * n - 256 : 256 * n] = (g * sigmoid(g) * u).astype(BF16)
         else:
             g, u = both[:, 0:128], both[:, 128:256]
-            hid[core, :, 512:640] = (g * sigmoid(g) * u).astype(BF16)
+            hid[span, 512:640] = (g * sigmoid(g) * u).astype(BF16)
             g = both[:, 256:384]
             u = pltpu.roll(g, 64, 1)
             lane = lax.broadcasted_iota(jnp.int32, g.shape, 1)
-            hid[core, :, 640:768] = jnp.where(lane < 64, g * sigmoid(g) * u, 0.0).astype(BF16)
+            hid[span, 640:768] = jnp.where(lane < 64, g * sigmoid(g) * u, 0.0).astype(BF16)
 
     def place(i):
         return (z + NF + (i + 1) // 2 * (1 - 2 * (i % 2))) % NF
 
-    def down(i, parts_of_k):
-        acc = jnp.zeros((NX * BLK, 256), F32)
-        for core in range(2):
-            for lanes in parts_of_k:
-                w = W[core, place(i), :, :, lanes]
-                acc = acc + dot_nt(hid[core, :, lanes], w.reshape(256, lanes.stop - lanes.start))
-        return acc
-
-    def down_first(i):
-        if i > 0:
-            came_from_partner(("PDA", (i + 1) // 2), W.at[c, 0 : 2 if i < 7 else 1, :, :, LANES["DA"]])
-        parts2[i] = down(i, (slice(0, 256), slice(512, 768)))
-
-    def down_last(i):
-        parts2[i] += down(i, (slice(256, 512),))
+    def down(i, rows, lanes):
+        w = W[place(i), :, :, lanes]
+        return dot_nt(hid[rows, lanes], w.reshape(256, lanes.stop - lanes.start))
+
+    def down_first(lo, hi):
+        for i in range(lo, hi):
+            parts2[i] = down(i, all_rows, slice(0, 256)) + down(i, all_rows, slice(512, 768))
+
+    def down_last(u, rows):
+        for i in range(*SPANS[u]):
+            parts2[i, rows] += down(i, rows, slice(256, 512))
+
+    SPANS = ((0, 4), (4, 7), (7, 8))
+
+    def pair_start(u):
+        span = slice(*SPANS[u])
+        psend[span] = parts2[span, other_rows, :].astype(BF16)
+        send(psend.at[span], pbuf.at[span], partner, ("h", u), ("h", u))
+
+    def pair_end(u):
+        span = slice(*SPANS[u])
+        arrived(("h", u), pbuf.at[span])
+        parts2[span, mine_rows, :] += pbuf[span].astype(F32)
 
     bufs0 = (rl0, rr0, fl0, fr0)
     bufs1 = (rl1, rr1, fl1, fr1)
 
     def take0(rel, half):
-        return parts2[0:3, BLK * rel : BLK * rel + BLK, 128 * half : 128 * half + 128]
+        return parts2[0:4, BLK * rel : BLK * rel + BLK, 128 * half : 128 * half + 128]
 
     def take1(rel, half):
-        return parts2[3:7, BLK * rel : BLK * rel + BLK, 128 * half : 128 * half + 128]
+        return parts2[4:7, BLK * rel : BLK * rel + BLK, 128 * half : 128 * half + 128]
 
     def g0s():
+        pair_end(0)
         scatter_start(1, take0, sb0, bufs0)
 
     def g0r():
         scatter_relay(1, take0, sb0, bufs0)
 
     def g1s():
+        pair_end(1)
         scatter_start(2, take1, sb1, bufs1)
 
     def g1r():
         scatter_relay(2, take1, sb1, bufs1)
 
     def g2s():
+        pair_end(2)
         for k, (rel, step) in enumerate(((2, 2), (1, 1), (3, NX - 1))):
             sb2[k] = parts2[7, BLK * rel : BLK * rel + BLK, :].astype(BF16)
             send(sb2.at[k], rb2.at[k], at_x(step), "d", "d")
@@ -493,14 +484,17 @@
     steps = {
         "scan1": scan1, "scan2": scan2, "scan3": scan3, "row": row, "col": col, "mix": mix, "mix2": mix2,
         "relay": relay, "send": norm_and_send, "ag": ag, "agend": agend, "g0s": g0s, "g0r": g0r, "g1s": g1s,
-        "g1r": g1r, "g2s": g2s,
+        "g1r": g1r, "g2s": g2s, "agp": agp, "ag2": ag2,
     }
-    for n in range(3):
-        for core in range(2):
-            steps["u%dc%d" % (n, core)] = functools.partial(gate_and_up, n, core)
-    for i in range(NF):
-        steps["e%d" % i] = functools.partial(down_first, i)
-        steps["f%d" % i] = functools.partial(down_last, i)
+    for n in range(2):
+        steps["u%d" % n] = functools.partial(gate_up, n, all_rows)
+    for n, span in enumerate(((0, 5), (5, 7), (7, 8))):
+        steps["e%d" % n] = functools.partial(down_first, *span)
+        steps["h%d" % n] = functools.partial(pair_start, n)
+    for name, rows in (("p", other_rows), ("o", mine_rows)):
+        steps["u2" + name] = functools.partial(gate_up, 2, rows)
+        for n in range(3):
+            steps["f%d" % n + name] = functools.partial(down_last, n, rows)
 
     for name, t, q in ORDER:
         if name in steps:
@@ -510,14 +504,6 @@
             hop1_done(fam, t)
             if t < 4:
                 hop1(fam, t + 1)
-            else:
-                ref = row_of(fam, second[fam], LA if fam == "A" else LB)
-                send(ref, ref, partner, "P0", "P0")
-            hop2("GA" if fam == "A" else "GB1", 1, t)
-        elif name[0] == "P":
-            to_partner(name[1:], t)
-        elif name[0] == "Q":
-            group_to_partner(name[1:], t, q)
         else:
             if t > 0:
                 hop2_done(name, t, q)
@@ -527,7 +513,7 @@
     def put(i, lane, value):
         ffn[:, pl.ds(pl.multiple_of(place(i) * 256 + lane, 128), value.shape[-1])] = value
 
-    for u, lo, hi, take_, sbuf, (_, _, fl_, fr_) in ((1, 0, 3, take0, sb0, bufs0), (2, 3, 7, take1, sb1, bufs1)):
+    for u, lo, hi, take_, sbuf, (_, _, fl_, fr_) in ((1, 0, 4, take0, sb0, bufs0), (2, 4, 7, take1, sb1, bufs1)):
         arrived(("f", u), sbuf.at[0:4])
         for half in range(2):
             got = take_(0, half) + fl_[half].astype(F32) + fr_[half].astype(F32)
@@ -538,17 +524,14 @@
     out[...] = (stream[...] + 0.5 * rms_scale(ffn[...], og[...])).astype(BF16)
 
     for fam, lanes in (("A", LA), ("B", LB)):
-        sent("S" + fam, W.at[c, 0, 0:7, :, lanes])
+        sent("S" + fam, W.at[0, 0:7, :, lanes])
     for name in LANES:
-        sent(name, W.at[c, 0:7, :, :, LANES[name]])
-    sent("P0", W.at[c, 0, :, :, ALL])
-    for name in ("GA", "GB1", "GB2"):
-        sent("P" + name, W.at[c, 0:7, :, :, LANES[name]])
-    for t, n in ((1, 2), (2, 2), (3, 2), (4, 1)):
-        sent(("PDA", t), W.at[c, 0:n, :, :, LANES["DA"]])
+        sent(name, W.at[0:7, :, :, LANES[name]])
+    for u, span in enumerate(SPANS):
+        sent(("h", u), psend.at[slice(*span)])
     for out_, ref in (
         ("halo", halo), ("wp", wp.at[1]), ("row", rowbuf), ("col", colbuf), ("mix", mixb), (("sb", 0), sb),
-        ("nb", sb), (("sb", 1), sb0), (("sb", 2), sb1), ("d", sb2),
+        ("nb", sb), ("nbp", nb.at[0]), (("sb", 1), sb0), (("sb", 2), sb1), ("d", sb2),
     ):
         sent(out_, ref)
     assert len(recv_ids) <= NRECV and len(send_ids) <= NSEND, (len(recv_ids), len(send_ids))
@@ -565,7 +548,7 @@
         in_specs=[pl.BlockSpec(memory_space=pl.ANY)] * 15,
         out_specs=pl.BlockSpec(memory_space=pltpu.VMEM),
         scratch_shapes=[
-            vmem((2, NF, NF, 32, WL), BF16),
+            vmem((NF, NF, 32, WL), BF16),
             vmem((2, CH, D), BF16),
             vmem((ROWS, CH), BF16),
             vmem((ROWS + 16, CH), F32),
@@ -603,19 +586,21 @@
             vmem((BLK, 1024), BF16),
             vmem((2, BLK, 1024), BF16),
             vmem((2, BLK, 1024), BF16),
-            vmem((2, NX, BLK, 1024), BF16),
-            vmem((2, NX * BLK, 768), BF16),
-            vmem((NF, NX * BLK, 256), F32),
+            vmem((2, 2 * NX, BLK, 1024), BF16),
+            vmem((2 * NX * BLK, 768), BF16),
+            vmem((NF, 2 * NX * BLK, 256), F32),
+            vmem((NF, NX * BLK, 256), BF16),
+            vmem((NF, NX * BLK, 256), BF16),
+            vmem((6, 4, BLK, 128), BF16),
+            vmem((4, BLK, 128), BF16),
+            vmem((4, BLK, 128), BF16),
+            vmem((2, 4, BLK, 128), BF16),
+            vmem((2, 4, BLK, 128), BF16),
             vmem((6, 3, BLK, 128), BF16),
             vmem((3, BLK, 128), BF16),
             vmem((3, BLK, 128), BF16),
             vmem((2, 3, BLK, 128), BF16),
             vmem((2, 3, BLK, 128), BF16),
-            vmem((6, 4, BLK, 128), BF16),
-            vmem((4, BLK, 128), BF16),
-            vmem((4, BLK, 128), BF16),
-            vmem((2, 4, BLK, 128), BF16),
-            vmem((2, 4, BLK, 128), BF16),
             vmem((3, BLK, 256), BF16),
             vmem((3, BLK, 256), BF16),
             vmem((BLK, D), F32),

time: 87.5 us -> 82.5 us (0.943)
  Pallas kernels: 85.7 us -> 80.7 us
    pallas_call x1, Pallas kernels: 85.7 us -> 80.7 us  [shards(): pl.pallas_call(kernel, out_shape=jax.ShapeDtypeStruct((BLK, D), BF16), in...]
where the time goes in v4:
time: 82.5 us; the launch traced here: 82.3 us
  Pallas kernels  80.7 us (98%)
  local copies, waits for them, and re-layouts  1.62 us (2%)
    pallas_call x1, Pallas kernels, shards(): pl.pallas_call(kernel, out_shape=jax.ShapeDtypeStruct((BLK, D), BF16), in...  80.7 us

profile of v4, /device:TPU:1, one launch (start us, length us, event | category | flops | bytes accessed | tf_op | source)
XLA Modules:
  0.0 82.3 jit_solution(15560269596480371764)
XLA Ops:
  0.0 80.7 %layer.1 = bf16[48,2048]{1,0:T(8,128)(2,1)} custom-call(bf16[384,2048]{1,0:T(8,128)(2,1)} %resid.1, bf16[384,256]{1,0:T(8,128)(2,1)} %x_in.1, bf16[384,256]{1,0:T(8,128)(2,1)} %g_in.1, f32[4,256]{1,0:T(4,128)} %conv_w.1, bf16[4,64,64]{2,1,0:T(8,128)(2,1)} %ga_in.1, bf16[4,64,64]{2,1,0:T(8,128)(2,1)} %gx_in.1, f32[1,256]{1,0:T(1,128)} %bitcast.9, ...), custom_call_target="tpu_custom_call" | custom-call | tf_op jit(solution)/shard_map/layer/pallas_call | solution.py:545
  80.7 1.6 %copy.17 = bf16[48,2048]{1,0:T(8,128)(2,1)} copy(bf16[48,2048]{1,0:T(8,128)(2,1)} %layer.1) | data formatting | bytes 393216

commit v5 on v4

--- a/solution.py
+++ b/solution.py
@@ -29,26 +29,26 @@
 
 ORDER = (
     ("GB1", 0, 0), ("GA", 0, 0), ("GB2", 0, 0), ("DA", 0, 0), ("scan1", 0, 0), ("SB", 1, 0), ("GB1", 0, 1),
-    ("SA", 1, 0), ("scan2", 0, 0), ("GA", 0, 1), ("scan3", 0, 0), ("GB1", 1, 0), ("GA", 1, 0), ("DA", 0, 1),
-    ("GB2", 0, 1), ("SB", 2, 0), ("GB1", 0, 2), ("GB1", 1, 1), ("SA", 2, 0), ("GA", 1, 1), ("GA", 2, 0),
-    ("GA", 0, 2), ("GB1", 2, 0), ("row", 0, 0), ("DA", 1, 0), ("SB", 3, 0), ("GB1", 0, 3), ("GA", 2, 1),
-    ("GB1", 1, 2), ("GA", 3, 0), ("GB1", 2, 1), ("GA", 1, 2), ("SA", 3, 0), ("GA", 0, 3), ("DA", 0, 2),
-    ("SB", 4, 0), ("GB1", 3, 0), ("GB1", 0, 4), ("col", 0, 0), ("GB1", 1, 3), ("GA", 3, 1), ("GA", 4, 0),
-    ("mix", 0, 0), ("GA", 2, 2), ("GB1", 2, 2), ("GA", 1, 3), ("mix2", 0, 0), ("GB1", 3, 1), ("SA", 4, 0),
-    ("GA", 0, 4), ("GB1", 4, 0), ("DA", 1, 1), ("GB1", 1, 4), ("GA", 4, 1), ("GB2", 1, 0), ("GB1", 2, 3),
-    ("GA", 3, 2), ("DA", 0, 3), ("GB1", 3, 2), ("relay", 0, 0), ("GB1", 4, 1), ("GB2", 0, 2), ("GA", 2, 3),
-    ("GB1", 2, 4), ("GA", 1, 4), ("GB2", 1, 1), ("GA", 4, 2), ("DA", 2, 0), ("GB1", 3, 3), ("GB1", 4, 2),
-    ("DA", 0, 4), ("send", 0, 0), ("GB2", 0, 3), ("DA", 1, 2), ("GB1", 3, 4), ("GA", 3, 3), ("GB2", 0, 4),
-    ("GA", 2, 4), ("GB2", 2, 0), ("GB2", 1, 2), ("GB1", 4, 3), ("DA", 2, 1), ("ag", 0, 0), ("GB2", 2, 1),
-    ("GB1", 4, 4), ("DA", 1, 3), ("GB2", 1, 3), ("GA", 4, 3), ("ag2", 0, 0), ("GA", 3, 4), ("GB2", 1, 4),
-    ("GB2", 3, 0), ("DA", 3, 0), ("GB2", 2, 2), ("DA", 1, 4), ("agend", 0, 0), ("DA", 2, 2), ("GB2", 3, 1),
-    ("GB2", 2, 3), ("agp", 0, 0), ("u1", 0, 0), ("DA", 3, 1), ("GB2", 2, 4), ("GA", 4, 4), ("GB2", 4, 0),
-    ("DA", 4, 0), ("u0", 0, 0), ("DA", 2, 3), ("GB2", 3, 2), ("GB2", 4, 1), ("DA", 2, 4), ("e0", 0, 0),
-    ("DA", 3, 2), ("GB2", 3, 3), ("GB2", 3, 4), ("DA", 4, 1), ("GB2", 4, 2), ("DA", 3, 3), ("GB2", 4, 3),
-    ("GB2", 4, 4), ("u2p", 0, 0), ("DA", 3, 4), ("f0p", 0, 0), ("e1", 0, 0), ("DA", 4, 2), ("h0", 0, 0),
-    ("f1p", 0, 0), ("h1", 0, 0), ("u2o", 0, 0), ("DA", 4, 3), ("f0o", 0, 0), ("DA", 4, 4), ("f1o", 0, 0),
-    ("g0s", 0, 0), ("e2", 0, 0), ("g1s", 0, 0), ("f2p", 0, 0), ("h2", 0, 0), ("f2o", 0, 0), ("g2s", 0, 0),
-    ("g0r", 0, 0), ("g1r", 0, 0),
+    ("SA", 1, 0), ("scan2", 0, 0), ("GA", 0, 1), ("scan3", 0, 0), ("GB1", 1, 0), ("GB2", 0, 1), ("GA", 1, 0),
+    ("DA", 0, 1), ("GB2", 1, 0), ("SB", 2, 0), ("GB1", 0, 2), ("SA", 2, 0), ("GA", 0, 2), ("GB1", 1, 1),
+    ("GA", 1, 1), ("GA", 2, 0), ("GB1", 2, 0), ("row", 0, 0), ("DA", 0, 2), ("SB", 3, 0), ("GB1", 0, 3),
+    ("GA", 1, 2), ("GB1", 1, 2), ("GA", 2, 1), ("SA", 3, 0), ("GA", 0, 3), ("GB1", 2, 1), ("GA", 3, 0),
+    ("DA", 0, 3), ("GB1", 3, 0), ("SB", 4, 0), ("GB1", 0, 4), ("col", 0, 0), ("mix", 0, 0), ("GB1", 1, 3),
+    ("GA", 2, 2), ("GB1", 2, 2), ("GA", 3, 1), ("SA", 4, 0), ("GA", 0, 4), ("mix2", 0, 0), ("DA", 0, 4),
+    ("GB2", 0, 2), ("GA", 1, 3), ("GB1", 3, 1), ("DA", 1, 0), ("GB1", 1, 4), ("GB2", 0, 3), ("DA", 1, 1),
+    ("relay", 0, 0), ("GB1", 2, 3), ("GA", 1, 4), ("GA", 3, 2), ("GB1", 3, 2), ("DA", 1, 2), ("GB2", 0, 4),
+    ("GB2", 1, 1), ("GA", 2, 3), ("GB1", 2, 4), ("send", 0, 0), ("GB2", 1, 2), ("DA", 1, 3), ("GB1", 3, 3),
+    ("GB2", 1, 3), ("GA", 2, 4), ("DA", 1, 4), ("GB2", 1, 4), ("DA", 2, 0), ("ag", 0, 0), ("GB2", 2, 0),
+    ("GA", 3, 3), ("GB1", 3, 4), ("GB2", 2, 1), ("DA", 2, 1), ("ag2", 0, 0), ("GB2", 2, 2), ("GA", 3, 4),
+    ("DA", 2, 2), ("GB2", 2, 3), ("agend", 0, 0), ("GB2", 2, 4), ("DA", 2, 3), ("GB2", 3, 0), ("agp", 0, 0),
+    ("GB1", 4, 0), ("GB1", 4, 1), ("GB1", 4, 2), ("GB1", 4, 3), ("GB1", 4, 4), ("u1", 0, 0), ("GB2", 3, 1),
+    ("DA", 2, 4), ("GA", 4, 0), ("GA", 4, 1), ("GA", 4, 2), ("GA", 4, 3), ("GA", 4, 4), ("u0", 0, 0), ("DA", 3, 0),
+    ("GB2", 3, 2), ("e0", 0, 0), ("DA", 3, 1), ("GB2", 3, 3), ("GB2", 3, 4), ("DA", 3, 2), ("DA", 3, 3),
+    ("DA", 3, 4), ("GB2", 4, 0), ("GB2", 4, 1), ("GB2", 4, 2), ("GB2", 4, 3), ("GB2", 4, 4), ("u2p", 0, 0),
+    ("f0p", 0, 0), ("h0", 0, 0), ("u2o", 0, 0), ("f0o", 0, 0), ("e1", 0, 0), ("f1p", 0, 0), ("h1", 0, 0),
+    ("g0s", 0, 0), ("f1o", 0, 0), ("DA", 4, 0), ("DA", 4, 1), ("DA", 4, 2), ("DA", 4, 3), ("DA", 4, 4),
+    ("e2", 0, 0), ("f2p", 0, 0), ("h2", 0, 0), ("g1s", 0, 0), ("f2o", 0, 0), ("g0r", 0, 0), ("g2s", 0, 0),
+    ("g1r", 0, 0),
 )
 
 
@@ -104,6 +104,13 @@
     partner = {"sp": sp, "tp": x * 2 + (1 - c)}
     behind = {"sp": (sp + NF * NF - 1) % (NF * NF), "tp": tp}
     ahead = {"sp": (sp + 1) % (NF * NF), "tp": tp}
+
+    barrier = pltpu.get_barrier_semaphore()
+    peers = [at_zy(z, (y + k) % NF) for k in range(1, NF)]
+    peers += [at_zy((z + k) % NF, y) for k in range(1, NF)]
+    peers += [at_x(1), at_x(2), at_x(NX - 1), partner, behind, ahead]
+    for peer in peers:
+        pl.semaphore_signal(barrier, inc=1, device_id=peer, device_id_type=MESH)
 
     loads = {}
 
@@ -127,13 +134,6 @@
     load("mg", mixg, mg)
     load("pg", preg, pg)
     load("og", outg, og)
-
-    barrier = pltpu.get_barrier_semaphore()
-    peers = [at_zy(z, (y + k) % NF) for k in range(1, NF)]
-    peers += [at_zy((z + k) % NF, y) for k in range(1, NF)]
-    peers += [at_x(1), at_x(2), at_x(NX - 1), partner, behind, ahead]
-    for peer in peers:
-        pl.semaphore_signal(barrier, inc=1, device_id=peer, device_id_type=MESH)
 
     for name in ("wg", "wu", "wd"):
         loads[name].wait()

time: 82.5 us -> 80.6 us (0.977)
  Pallas kernels: 80.7 us -> 78.8 us
    pallas_call x1, Pallas kernels: 80.7 us -> 78.8 us  [shards(): pl.pallas_call(kernel, out_shape=jax.ShapeDtypeStruct((BLK, D), BF16), in...]
where the time goes in v5:
time: 80.6 us; the launch traced here: 80.5 us
  Pallas kernels  78.8 us (98%)
  local copies, waits for them, and re-layouts  1.62 us (2%)
    pallas_call x1, Pallas kernels, shards(): pl.pallas_call(kernel, out_shape=jax.ShapeDtypeStruct((BLK, D), BF16), in...  78.8 us
    unnamed x1, local copies, waits for them, and re-layouts  1.62 us

profile of v5, /device:TPU:1, one launch (start us, length us, event | category | flops | bytes accessed | tf_op | source)
XLA Modules:
  0.0 80.5 jit_solution(14311088348780828346)
XLA Ops:
  0.0 78.8 %layer.1 = bf16[48,2048]{1,0:T(8,128)(2,1)} custom-call(bf16[384,2048]{1,0:T(8,128)(2,1)} %resid.1, bf16[384,256]{1,0:T(8,128)(2,1)} %x_in.1, bf16[384,256]{1,0:T(8,128)(2,1)} %g_in.1, f32[4,256]{1,0:T(4,128)} %conv_w.1, bf16[4,64,64]{2,1,0:T(8,128)(2,1)} %ga_in.1, bf16[4,64,64]{2,1,0:T(8,128)(2,1)} %gx_in.1, f32[1,256]{1,0:T(1,128)} %bitcast.9, ...), custom_call_target="tpu_custom_call" | custom-call | tf_op jit(solution)/shard_map/layer/pallas_call | solution.py:545
  78.9 1.6 %copy.17 = bf16[48,2048]{1,0:T(8,128)(2,1)} copy(bf16[48,2048]{1,0:T(8,128)(2,1)} %layer.1) | data formatting | bytes 393216

commit v6 on v5

--- a/solution.py
+++ b/solution.py
@@ -45,8 +45,8 @@
     ("DA", 2, 4), ("GA", 4, 0), ("GA", 4, 1), ("GA", 4, 2), ("GA", 4, 3), ("GA", 4, 4), ("u0", 0, 0), ("DA", 3, 0),
     ("GB2", 3, 2), ("e0", 0, 0), ("DA", 3, 1), ("GB2", 3, 3), ("GB2", 3, 4), ("DA", 3, 2), ("DA", 3, 3),
     ("DA", 3, 4), ("GB2", 4, 0), ("GB2", 4, 1), ("GB2", 4, 2), ("GB2", 4, 3), ("GB2", 4, 4), ("u2p", 0, 0),
-    ("f0p", 0, 0), ("h0", 0, 0), ("u2o", 0, 0), ("f0o", 0, 0), ("e1", 0, 0), ("f1p", 0, 0), ("h1", 0, 0),
-    ("g0s", 0, 0), ("f1o", 0, 0), ("DA", 4, 0), ("DA", 4, 1), ("DA", 4, 2), ("DA", 4, 3), ("DA", 4, 4),
+    ("f0p", 0, 0), ("h0", 0, 0), ("e1", 0, 0), ("f1p", 0, 0), ("h1", 0, 0), ("u2o", 0, 0), ("f0o", 0, 0),
+    ("f1o", 0, 0), ("g0s", 0, 0), ("DA", 4, 0), ("DA", 4, 1), ("DA", 4, 2), ("DA", 4, 3), ("DA", 4, 4),
     ("e2", 0, 0), ("f2p", 0, 0), ("h2", 0, 0), ("g1s", 0, 0), ("f2o", 0, 0), ("g0r", 0, 0), ("g2s", 0, 0),
     ("g1r", 0, 0),
 )

time: 80.6 us -> 79.7 us (0.989)
  Pallas kernels: 78.8 us -> 77.9 us
    pallas_call x1, Pallas kernels: 78.8 us -> 77.9 us  [shards(): pl.pallas_call(kernel, out_shape=jax.ShapeDtypeStruct((BLK, D), BF16), in...]
where the time goes in v6:
time: 79.7 us; the launch traced here: 79.6 us
  Pallas kernels  77.9 us (98%)
  local copies, waits for them, and re-layouts  1.62 us (2%)
    pallas_call x1, Pallas kernels, shards(): pl.pallas_call(kernel, out_shape=jax.ShapeDtypeStruct((BLK, D), BF16), in...  77.9 us
    unnamed x1, local copies, waits for them, and re-layouts  1.62 us

profile of v6, /device:TPU:1, one launch (start us, length us, event | category | flops | bytes accessed | tf_op | source)
XLA Modules:
  0.0 79.6 jit_solution(4014566075791066002)
XLA Ops:
  0.0 77.9 %layer.1 = bf16[48,2048]{1,0:T(8,128)(2,1)} custom-call(bf16[384,2048]{1,0:T(8,128)(2,1)} %resid.1, bf16[384,256]{1,0:T(8,128)(2,1)} %x_in.1, bf16[384,256]{1,0:T(8,128)(2,1)} %g_in.1, f32[4,256]{1,0:T(4,128)} %conv_w.1, bf16[4,64,64]{2,1,0:T(8,128)(2,1)} %ga_in.1, bf16[4,64,64]{2,1,0:T(8,128)(2,1)} %gx_in.1, f32[1,256]{1,0:T(1,128)} %bitcast.9, ...), custom_call_target="tpu_custom_call" | custom-call | tf_op jit(solution)/shard_map/layer/pallas_call | solution.py:545
  77.9 1.6 %copy.17 = bf16[48,2048]{1,0:T(8,128)(2,1)} copy(bf16[48,2048]{1,0:T(8,128)(2,1)} %layer.1) | data formatting | bytes 393216

commit v7 on v6

--- a/solution.py
+++ b/solution.py
@@ -29,26 +29,26 @@
 
 ORDER = (
     ("GB1", 0, 0), ("GA", 0, 0), ("GB2", 0, 0), ("DA", 0, 0), ("scan1", 0, 0), ("SB", 1, 0), ("GB1", 0, 1),
-    ("SA", 1, 0), ("scan2", 0, 0), ("GA", 0, 1), ("scan3", 0, 0), ("GB1", 1, 0), ("GB2", 0, 1), ("GA", 1, 0),
-    ("DA", 0, 1), ("GB2", 1, 0), ("SB", 2, 0), ("GB1", 0, 2), ("SA", 2, 0), ("GA", 0, 2), ("GB1", 1, 1),
-    ("GA", 1, 1), ("GA", 2, 0), ("GB1", 2, 0), ("row", 0, 0), ("DA", 0, 2), ("SB", 3, 0), ("GB1", 0, 3),
-    ("GA", 1, 2), ("GB1", 1, 2), ("GA", 2, 1), ("SA", 3, 0), ("GA", 0, 3), ("GB1", 2, 1), ("GA", 3, 0),
-    ("DA", 0, 3), ("GB1", 3, 0), ("SB", 4, 0), ("GB1", 0, 4), ("col", 0, 0), ("mix", 0, 0), ("GB1", 1, 3),
-    ("GA", 2, 2), ("GB1", 2, 2), ("GA", 3, 1), ("SA", 4, 0), ("GA", 0, 4), ("mix2", 0, 0), ("DA", 0, 4),
-    ("GB2", 0, 2), ("GA", 1, 3), ("GB1", 3, 1), ("DA", 1, 0), ("GB1", 1, 4), ("GB2", 0, 3), ("DA", 1, 1),
-    ("relay", 0, 0), ("GB1", 2, 3), ("GA", 1, 4), ("GA", 3, 2), ("GB1", 3, 2), ("DA", 1, 2), ("GB2", 0, 4),
-    ("GB2", 1, 1), ("GA", 2, 3), ("GB1", 2, 4), ("send", 0, 0), ("GB2", 1, 2), ("DA", 1, 3), ("GB1", 3, 3),
-    ("GB2", 1, 3), ("GA", 2, 4), ("DA", 1, 4), ("GB2", 1, 4), ("DA", 2, 0), ("ag", 0, 0), ("GB2", 2, 0),
-    ("GA", 3, 3), ("GB1", 3, 4), ("GB2", 2, 1), ("DA", 2, 1), ("ag2", 0, 0), ("GB2", 2, 2), ("GA", 3, 4),
-    ("DA", 2, 2), ("GB2", 2, 3), ("agend", 0, 0), ("GB2", 2, 4), ("DA", 2, 3), ("GB2", 3, 0), ("agp", 0, 0),
+    ("SA", 1, 0), ("scan2", 0, 0), ("GA", 0, 1), ("scan3", 0, 0), ("GB1", 1, 0), ("GA", 1, 0), ("GB2", 0, 1),
+    ("DA", 0, 1), ("GB2", 1, 0), ("SB", 2, 0), ("GB1", 0, 2), ("GB1", 1, 1), ("SA", 2, 0), ("GA", 0, 2),
+    ("GA", 1, 1), ("GB1", 2, 0), ("GA", 2, 0), ("row", 0, 0), ("DA", 0, 2), ("SB", 3, 0), ("GB1", 0, 3),
+    ("GA", 1, 2), ("GB1", 1, 2), ("GA", 2, 1), ("GB1", 2, 1), ("GA", 3, 0), ("DA", 1, 0), ("SA", 3, 0),
+    ("GA", 0, 3), ("GB1", 3, 0), ("SB", 4, 0), ("GB1", 0, 4), ("col", 0, 0), ("DA", 0, 3), ("GB1", 1, 3),
+    ("mix", 0, 0), ("GB1", 2, 2), ("GA", 2, 2), ("mix2", 0, 0), ("GA", 3, 1), ("GB1", 3, 1), ("DA", 1, 1),
+    ("SA", 4, 0), ("GB2", 0, 2), ("GB1", 1, 4), ("GA", 0, 4), ("GA", 1, 3), ("GB2", 0, 3), ("GB1", 2, 3),
+    ("DA", 0, 4), ("relay", 0, 0), ("GA", 3, 2), ("DA", 1, 2), ("GB1", 3, 2), ("GB2", 0, 4), ("GB2", 1, 1),
+    ("GA", 1, 4), ("GB1", 2, 4), ("DA", 1, 3), ("send", 0, 0), ("GB2", 1, 2), ("GA", 2, 3), ("GB1", 3, 3),
+    ("GB2", 1, 3), ("DA", 1, 4), ("DA", 2, 0), ("GB2", 1, 4), ("GA", 2, 4), ("ag", 0, 0), ("GB2", 2, 0),
+    ("DA", 2, 1), ("GB1", 3, 4), ("GB2", 2, 1), ("ag2", 0, 0), ("GB2", 2, 2), ("GA", 3, 3), ("DA", 2, 2),
+    ("GB2", 2, 3), ("agend", 0, 0), ("GB2", 2, 4), ("GA", 3, 4), ("DA", 2, 3), ("GB2", 3, 0), ("agp", 0, 0),
     ("GB1", 4, 0), ("GB1", 4, 1), ("GB1", 4, 2), ("GB1", 4, 3), ("GB1", 4, 4), ("u1", 0, 0), ("GB2", 3, 1),
-    ("DA", 2, 4), ("GA", 4, 0), ("GA", 4, 1), ("GA", 4, 2), ("GA", 4, 3), ("GA", 4, 4), ("u0", 0, 0), ("DA", 3, 0),
-    ("GB2", 3, 2), ("e0", 0, 0), ("DA", 3, 1), ("GB2", 3, 3), ("GB2", 3, 4), ("DA", 3, 2), ("DA", 3, 3),
-    ("DA", 3, 4), ("GB2", 4, 0), ("GB2", 4, 1), ("GB2", 4, 2), ("GB2", 4, 3), ("GB2", 4, 4), ("u2p", 0, 0),
-    ("f0p", 0, 0), ("h0", 0, 0), ("e1", 0, 0), ("f1p", 0, 0), ("h1", 0, 0), ("u2o", 0, 0), ("f0o", 0, 0),
-    ("f1o", 0, 0), ("g0s", 0, 0), ("DA", 4, 0), ("DA", 4, 1), ("DA", 4, 2), ("DA", 4, 3), ("DA", 4, 4),
-    ("e2", 0, 0), ("f2p", 0, 0), ("h2", 0, 0), ("g1s", 0, 0), ("f2o", 0, 0), ("g0r", 0, 0), ("g2s", 0, 0),
-    ("g1r", 0, 0),
+    ("DA", 2, 4), ("GB2", 3, 2), ("DA", 3, 0), ("DA", 3, 1), ("GB2", 3, 3), ("GA", 4, 0), ("GA", 4, 1),
+    ("GA", 4, 2), ("GA", 4, 3), ("GA", 4, 4), ("u0", 0, 0), ("DA", 3, 2), ("GB2", 3, 4), ("e0", 0, 0),
+    ("DA", 3, 3), ("DA", 3, 4), ("GB2", 4, 0), ("GB2", 4, 1), ("GB2", 4, 2), ("GB2", 4, 3), ("GB2", 4, 4),
+    ("u2p", 0, 0), ("f0p", 0, 0), ("h0", 0, 0), ("e1", 0, 0), ("f1p", 0, 0), ("h1", 0, 0), ("u2o", 0, 0),
+    ("f0o", 0, 0), ("f1o", 0, 0), ("g0s", 0, 0), ("DA", 4, 0), ("DA", 4, 1), ("DA", 4, 2), ("DA", 4, 3),
+    ("DA", 4, 4), ("e2", 0, 0), ("f2p", 0, 0), ("h2", 0, 0), ("g1s", 0, 0), ("f2o", 0, 0), ("g0r", 0, 0),
+    ("g2s", 0, 0), ("g1r", 0, 0),
 )
 
 

time: 79.7 us -> 79.9 us (level)
  no operation moved by 1% of the time
where the time goes in v7:
time: 79.9 us; the launch traced here: 79.7 us
  Pallas kernels  78.1 us (98%)
  local copies, waits for them, and re-layouts  1.62 us (2%)
    pallas_call x1, Pallas kernels, shards(): pl.pallas_call(kernel, out_shape=jax.ShapeDtypeStruct((BLK, D), BF16), in...  78.1 us
    unnamed x1, local copies, waits for them, and re-layouts  1.62 us

profile of v7, /device:TPU:1, one launch (start us, length us, event | category | flops | bytes accessed | tf_op | source)
XLA Modules:
  0.0 79.7 jit_solution(12143979485189681875)
XLA Ops:
  0.0 78.1 %layer.1 = bf16[48,2048]{1,0:T(8,128)(2,1)} custom-call(bf16[384,2048]{1,0:T(8,128)(2,1)} %resid.1, bf16[384,256]{1,0:T(8,128)(2,1)} %x_in.1, bf16[384,256]{1,0:T(8,128)(2,1)} %g_in.1, f32[4,256]{1,0:T(4,128)} %conv_w.1, bf16[4,64,64]{2,1,0:T(8,128)(2,1)} %ga_in.1, bf16[4,64,64]{2,1,0:T(8,128)(2,1)} %gx_in.1, f32[1,256]{1,0:T(1,128)} %bitcast.9, ...), custom_call_target="tpu_custom_call" | custom-call | tf_op jit(solution)/shard_map/layer/pallas_call | solution.py:545
  78.1 1.6 %copy.17 = bf16[48,2048]{1,0:T(8,128)(2,1)} copy(bf16[48,2048]{1,0:T(8,128)(2,1)} %layer.1) | data formatting | bytes 393216
